TPU v7x, 32 devices: a whole 2x2x4 slice. The times are simulated.
32 devices in a mesh: rep: 2 (over x), fs: 8 (over z, y), tp: 2 (over core).
Axes of the slice: x: 2, y: 2, z: 4, core: 2. Of those that a mesh axis runs over, the one named last changes fastest.
Arguments:
- later_input: bfloat16 [2048, 2048], P(('rep', 'fs')), may hold values from -6 to 6
- earlier_input: bfloat16 [2048, 2048], P(('rep', 'fs')), may hold values from -6 to 6
- cotangent: bfloat16 [2048, 2048], P(('rep', 'fs')), may hold values from -6 to 6
- gate_weight: bfloat16 [2048, 3072], P('fs', 'tp'), may hold values from -0.125 to 0.125
- up_weight: bfloat16 [2048, 3072], P('fs', 'tp'), may hold values from -0.125 to 0.125
- down_weight: bfloat16 [2048, 3072], P('fs', 'tp'), may hold values from -0.109375 to 0.109375
- gate_sum: float32 [2048, 3072], P('fs', 'tp'), may hold values from -192 to 192
- up_sum: float32 [2048, 3072], P('fs', 'tp'), may hold values from -192 to 192
- down_sum: float32 [2048, 3072], P('fs', 'tp'), may hold values from -192 to 192
Outputs:
- later_output: bfloat16 [2048, 2048], P(('rep', 'fs'))
- earlier_input_grad: bfloat16 [2048, 2048], P(('rep', 'fs'))
- gate_sum_new: float32 [2048, 3072], P('fs', 'tp')
- up_sum_new: float32 [2048, 3072], P('fs', 'tp')
- down_sum_new: float32 [2048, 3072], P('fs', 'tp')
All inputs are finite; a program needn't handle non-finite values.
Results may differ from a plain program's by a relative error of at most 0.02.
Values may be sent and summed in bfloat16 or wider, within the bound.
A program may use at most 128 MiB of HBM per device.

v0:
```python
import functools

import jax
import jax.numpy as jnp
from jax import lax
from jax.experimental import pallas as pl
from jax.experimental.pallas import tpu as pltpu
from jax.sharding import PartitionSpec as P

MESH = pl.DeviceIdType.MESH


def ring_position(index, n):
    side, height = lax.rem(index, 2), index // 2
    return (1 - side) * height + side * (n - 1 - height)


def ring_index(position, n):
    position = lax.rem(position + 2 * n, n)
    back = position // (n // 2)
    return (1 - back) * (2 * position) + back * (2 * (n - 1 - position) + 1)


def span(start, size, step):
    return pl.ds(pl.multiple_of(start, step), size)


def remote(source, target, send, recv, device):
    return pltpu.make_async_remote_copy(
        src_ref=source,
        dst_ref=target,
        send_sem=send,
        recv_sem=recv,
        device_id=device,
        device_id_type=MESH,
    )


def meet(n, r, f, t):
    barrier = pltpu.get_barrier_semaphore()
    for k in range(1, n):
        pl.semaphore_signal(barrier, inc=1, device_id={"fs": lax.rem(f + k, n)}, device_id_type=MESH)
    pl.semaphore_signal(barrier, inc=1, device_id={"rep": 1 - r}, device_id_type=MESH)
    pl.semaphore_signal(barrier, inc=1, device_id={"tp": 1 - t}, device_id_type=MESH)
    pl.semaphore_wait(barrier, n + 1)


def fused_kernel(
    n, tok, wt, late_out, early_out, g_out,
    slots, w, part, peer, acc, grads, ring_in, ring_out, x_in, x_out,
    ags, agr, aps, apr, ws, wr, wxs, wxr,
    ts, tr, rs, rr, os_, or_, xs, xr, gs, gr, fs_, fr,
):
    r, f, t = lax.axis_index("rep"), lax.axis_index("fs"), lax.axis_index("tp")
    m = tok.shape[1]
    q = m // 4
    hid, dl = wt.shape[1] // n, wt.shape[2]
    hl = dl // 2
    width = tok.shape[2]
    pos = ring_position(f, n)
    ahead = (ring_index(pos + 1, n), ring_index(pos - 1, n))
    outs = (late_out, early_out)
    f32, bf16 = jnp.float32, jnp.bfloat16
    meet(n, r, f, t)

    pending = []

    def go(copy):
        copy.start()
        pending.append(copy)

    def quarter(core, d):
        return span(core * (2 * q) + d * q, q, q)

    def half(core):
        return span(core * (2 * q), 2 * q, 2 * q)

    def piece(origin, side):
        return w.at[:, :, span(origin * dl + side * hl, hl, hl)]

    def along(s, d):
        block = slots.at[s, :, quarter(t, d), :]
        return remote(block, slots.at[s + 1, :, quarter(t, d), :], ags.at[d, s], agr.at[d, s], {"fs": ahead[d]})

    def arrived(s, d):
        block = slots.at[s, :, quarter(t, d), :]
        return remote(block, block, ags.at[d, s - 1], agr.at[d, s - 1], {"fs": ahead[d]})

    def across(s, d, core):
        block = slots.at[s, :, quarter(core, d), :]
        return remote(block, block, aps.at[d, s - 1], apr.at[d, s - 1], {"tp": 1 - t})

    def take_on(s):
        for d in range(2):
            arrived(s, d).wait_recv()

            @pl.when(s < n - 1)
            def _():
                along(s, d).start()

            across(s, d, t).start()

    for k in range(1, n):
        g = lax.rem(f + k, n)
        go(remote(
            wt.at[:, span(g * hid, hid, hid), span(r * hl, hl, hl)],
            piece(f, r), ws.at[k - 1], wr.at[k - 1], {"fs": g},
        ))
    for d in range(2):
        go(remote(tok.at[:, quarter(t, d), :], slots.at[1, :, quarter(t, d), :], ags.at[d, 0], agr.at[d, 0], {"fs": ahead[d]}))
    slots[0] = tok[...]
    w[:, :, span(f * dl, dl, dl)] = wt[:, span(f * hid, hid, hid), :]
    acc[...] = jnp.zeros_like(acc)
    for k in range(1, n):
        origin = lax.rem(f - k + n, n)
        block = piece(origin, r)
        remote(block, block, ws.at[k - 1], wr.at[k - 1], {"fs": origin}).wait_recv()
        go(remote(block, block, wxs.at[k - 1], wxr.at[k - 1], {"rep": 1 - r}))
    take_on(1)
    for k in range(1, n):
        block = piece(lax.rem(f - k + n, n), 1 - r)
        remote(block, block, wxs.at[k - 1], wxr.at[k - 1], {"rep": 1 - r}).wait_recv()

    step = width // 4

    def compute(s):
        pair = slots[s, 0:2].reshape(2 * m, width)
        gate, up = contract_last(pair, w[0]), contract_last(pair, w[1])
        hidden_late = (jax.nn.silu(gate[:m]) * up[:m]).astype(bf16)
        hidden_grad = contract_last(slots[s, 2], w[2])
        gate_grad, up_grad, hidden_early = early_parts(gate[m:], up[m:], hidden_grad)
        for c in range(4):
            lanes = slice(c * step, (c + 1) * step)
            part[s, 0, :, lanes] = jnp.dot(hidden_late, w[2, :, lanes], preferred_element_type=f32).astype(bf16)
            part[s, 1, :, lanes] = (
                jnp.dot(gate_grad, w[0, :, lanes], preferred_element_type=f32)
                + jnp.dot(up_grad, w[1, :, lanes], preferred_element_type=f32)
            ).astype(bf16)
            early = slots[s, 1, :, lanes]
            acc[0, :, lanes] += contract_first(gate_grad, early)
            acc[1, :, lanes] += contract_first(up_grad, early)
            acc[2, :, lanes] += contract_first(hidden_early, slots[s, 2, :, lanes])

    def trade(s):
        return remote(part.at[s, :, half(1 - t), :], peer.at[s], ts.at[s], tr.at[s], {"tp": 1 - t})

    def ring_step(s, carry):
        @pl.when(s > 1)
        def _():
            take_on(s)

        @pl.when(s > 1)
        def _():
            for d in range(2):
                across(s - 1, d, 1 - t).wait_recv()

        compute(s - 1)
        trade(s - 1).start()
        return carry

    lax.fori_loop(1, n, ring_step, 0)

    def own(s, o, d):
        return (
            part[s, o, quarter(t, d), :].astype(f32)
            + peer[s, o, d * q:(d + 1) * q, :].astype(f32)
        )

    def trade_done(s):
        remote(peer.at[s], peer.at[s], ts.at[s], tr.at[s], {"tp": 1 - t}).wait_recv()

    def sum_step(s):
        trade_done(s + 1)
        for o in range(2):
            for d in range(2):
                value = own(s + 1, o, d)
                if s > 0:
                    slot = ring_in.at[d, s - 1, o]
                    remote(slot, slot, rs.at[d, s - 1, o], rr.at[d, s - 1, o], {"fs": ahead[d]}).wait_recv()
                    value = value + ring_in[d, s - 1, o].astype(f32)
                ring_out[d, s, o] = value.astype(bf16)
                go(remote(ring_out.at[d, s, o], ring_in.at[d, s, o], rs.at[d, s, o], rr.at[d, s, o], {"fs": ahead[d]}))

    sum_step(0)
    for d in range(2):
        across(n - 1, d, 1 - t).wait_recv()
    compute(n - 1)
    trade(n - 1).start()
    grads[...] = acc[...].astype(bf16)
    order = list(range(1, n)) + [0]
    for k in order:
        g = lax.rem(f + k, n)
        go(remote(grads.at[:, :, span(g * dl + (1 - r) * hl, hl, hl)], x_in.at[k], xs.at[k], xr.at[k], {"rep": 1 - r}))

    def g_block(origin, side):
        return g_out.at[:, span(origin * hid, hid, hid), span(side * hl, hl, hl)]

    def pair_sum(k):
        g = lax.rem(f + k, n)
        remote(x_in.at[k], x_in.at[k], xs.at[k], xr.at[k], {"rep": 1 - r}).wait_recv()
        return (x_in[k].astype(f32) + acc[:, :, span(g * dl + r * hl, hl, hl)]).astype(bf16)

    def pass_on(k):
        origin = lax.rem(f - k + n, n)
        block = g_block(origin, r)
        remote(block, block, gs.at[k - 1], gr.at[k - 1], {"fs": origin}).wait_recv()
        go(remote(block, block, fs_.at[k], fr.at[k], {"rep": 1 - r}))

    for s in range(n - 1):
        if s > 0:
            sum_step(s)
        x_out[s] = pair_sum(s + 1)
        go(remote(x_out.at[s], g_block(f, r), gs.at[s], gr.at[s], {"fs": lax.rem(f + s + 1, n)}))
        if s >= 1:
            pass_on(s)
    g_out[:, span(f * hid, hid, hid), span(r * hl, hl, hl)] = pair_sum(0)
    block = g_block(f, r)
    go(remote(block, block, fs_.at[0], fr.at[0], {"rep": 1 - r}))
    trade_done(0)
    for o in range(2):
        for d in range(2):
            slot = ring_in.at[d, n - 2, o]
            remote(slot, slot, rs.at[d, n - 2, o], rr.at[d, n - 2, o], {"fs": ahead[d]}).wait_recv()
            value = own(0, o, d) + ring_in[d, n - 2, o].astype(f32)
            outs[o][quarter(t, d), :] = value.astype(bf16)
        mine = outs[o].at[half(t), :]
        go(remote(mine, mine, os_.at[o], or_.at[o], {"tp": 1 - t}))
    for k in range(n - 1, n):
        pass_on(k)
    for o in range(2):
        other = outs[o].at[half(1 - t), :]
        remote(other, other, os_.at[o], or_.at[o], {"tp": 1 - t}).wait_recv()
    for k in range(n):
        block = g_block(lax.rem(f - k + n, n), 1 - r)
        remote(block, block, fs_.at[k], fr.at[k], {"rep": 1 - r}).wait_recv()
    for s in range(n):
        trade(s).wait_send()
    for s in range(1, n):
        for d in range(2):
            if s < n - 1:
                along(s, d).wait_send()
            across(s, d, t).wait_send()
    for copy in pending:
        copy.wait_send()


def add_kernel(total, first, second, third, first_new, second_new, third_new):
    for i, (old, new) in enumerate(((first, first_new), (second, second_new), (third, third_new))):
        new[...] = old[...] + total[i].astype(jnp.float32).T


def add_turned(total, sums):
    _, ff, dl = total.shape
    width = 256
    block = pl.BlockSpec((dl, width), lambda i: (0, i))
    return pl.pallas_call(
        add_kernel,
        grid=(ff // width,),
        out_shape=tuple(jax.ShapeDtypeStruct(old.shape, old.dtype) for old in sums),
        in_specs=[pl.BlockSpec((3, width, dl), lambda i: (0, i, 0))] + [block] * 3,
        out_specs=(block,) * 3,
        name="add_turned",
    )(total, *sums)


VMEM = pl.BlockSpec(memory_space=pltpu.VMEM)


def dma(*shape):
    return pltpu.SemaphoreType.DMA(shape)


def split_hidden(
    n,
    later_input,
    earlier_input,
    cotangent,
    gate_weight,
    up_weight,
    down_weight,
    gate_sum,
    up_sum,
    down_sum,
):
    bf16 = jnp.bfloat16
    m, width = later_input.shape
    dl, ff = gate_weight.shape
    hid = ff // n
    hl, q = dl // 2, m // 4
    tokens = jnp.stack([later_input, earlier_input, cotangent])
    weights = jnp.stack([gate_weight.T, up_weight.T, down_weight.T])
    later_output, earlier_input_grad, total = pl.pallas_call(
        functools.partial(fused_kernel, n),
        out_shape=(
            jax.ShapeDtypeStruct((m, width), bf16),
            jax.ShapeDtypeStruct((m, width), bf16),
            jax.ShapeDtypeStruct((3, ff, dl), bf16),
        ),
        in_specs=[VMEM] * 2,
        out_specs=(VMEM, VMEM, VMEM),
        scratch_shapes=[
            pltpu.VMEM((n, 3, m, width), bf16),
            pltpu.VMEM((3, hid, width), bf16),
            pltpu.VMEM((n, 2, m, width), bf16),
            pltpu.VMEM((n, 2, 2 * q, width), bf16),
            pltpu.VMEM((3, hid, width), jnp.float32),
            pltpu.VMEM((3, hid, width), bf16),
            pltpu.VMEM((2, n - 1, 2, q, width), bf16),
            pltpu.VMEM((2, n - 1, 2, q, width), bf16),
            pltpu.VMEM((n, 3, hid, hl), bf16),
            pltpu.VMEM((n - 1, 3, hid, hl), bf16),
        ]
        + [dma(2, n - 1)] * 4
        + [dma(n - 1)] * 4
        + [
            dma(n), dma(n),
            dma(2, n - 1, 2), dma(2, n - 1, 2),
            dma(2), dma(2),
            dma(n), dma(n),
            dma(n - 1), dma(n - 1),
            dma(n), dma(n),
        ],
        compiler_params=pltpu.CompilerParams(
            collective_id=0, has_side_effects=True, vmem_limit_bytes=67043328
        ),
        name="fused",
    )(tokens, weights)
    return (later_output, earlier_input_grad) + tuple(add_turned(total, (gate_sum, up_sum, down_sum)))


def early_parts(gate_early, up_early, hidden_grad):
    sigmoid_gate = jax.nn.sigmoid(gate_early)
    silu_early = gate_early * sigmoid_gate
    gate_grad = (
        hidden_grad * up_early * sigmoid_gate * (1.0 + gate_early * (1.0 - sigmoid_gate))
    ).astype(jnp.bfloat16)
    up_grad = (hidden_grad * silu_early).astype(jnp.bfloat16)
    hidden_early = (silu_early * up_early).astype(jnp.bfloat16)
    return gate_grad, up_grad, hidden_early


def contract_last(first, second):
    return lax.dot_general(
        first, second, (((1,), (1,)), ((), ())), preferred_element_type=jnp.float32
    )


def contract_first(first, second):
    return lax.dot_general(
        first, second, (((0,), (0,)), ((), ())), preferred_element_type=jnp.float32
    )


def per_device(
    later_input,
    earlier_input,
    cotangent,
    gate_weight,
    up_weight,
    down_weight,
    gate_sum,
    up_sum,
    down_sum,
):
    gate_full, up_full, down_full = (
        lax.all_gather(gate_weight, "fs", axis=0, tiled=True),
        lax.all_gather(up_weight, "fs", axis=0, tiled=True),
        lax.all_gather(down_weight, "fs", axis=0, tiled=True),
    )
    gate_late = jnp.dot(later_input, gate_full, preferred_element_type=jnp.float32)
    up_late = jnp.dot(later_input, up_full, preferred_element_type=jnp.float32)
    hidden_late = (jax.nn.silu(gate_late) * up_late).astype(jnp.bfloat16)
    partial_late = contract_last(hidden_late, down_full)
    later_output = lax.psum(partial_late.astype(jnp.bfloat16), "tp")
    gate_early = jnp.dot(earlier_input, gate_full, preferred_element_type=jnp.float32)
    up_early = jnp.dot(earlier_input, up_full, preferred_element_type=jnp.float32)
    hidden_grad = jnp.dot(cotangent, down_full, preferred_element_type=jnp.float32)
    sigmoid_gate = jax.nn.sigmoid(gate_early)
    silu_early = gate_early * sigmoid_gate
    gate_grad = (
        hidden_grad * up_early * sigmoid_gate * (1.0 + gate_early * (1.0 - sigmoid_gate))
    ).astype(jnp.bfloat16)
    up_grad = (hidden_grad * silu_early).astype(jnp.bfloat16)
    hidden_early = (silu_early * up_early).astype(jnp.bfloat16)
    partial_early = contract_last(gate_grad, gate_full) + contract_last(up_grad, up_full)
    earlier_input_grad = lax.psum(partial_early.astype(jnp.bfloat16), "tp")
    columns, cot_columns = (
        lax.all_to_all(earlier_input, "fs", split_axis=1, concat_axis=0, tiled=True),
        lax.all_to_all(cotangent, "fs", split_axis=1, concat_axis=0, tiled=True),
    )
    gate_local = contract_first(columns, lax.all_gather(gate_grad, "fs", axis=0, tiled=True))
    up_local = contract_first(columns, lax.all_gather(up_grad, "fs", axis=0, tiled=True))
    down_local = contract_first(cot_columns, lax.all_gather(hidden_early, "fs", axis=0, tiled=True))
    gate_total, up_total, down_total = (
        lax.psum(gate_local.astype(jnp.bfloat16), "rep").astype(jnp.float32),
        lax.psum(up_local.astype(jnp.bfloat16), "rep").astype(jnp.float32),
        lax.psum(down_local.astype(jnp.bfloat16), "rep").astype(jnp.float32),
    )
    return (
        later_output,
        earlier_input_grad,
        gate_sum + gate_total,
        up_sum + up_total,
        down_sum + down_total,
    )


def solution(mesh):
    placed = (
        P(("rep", "fs"), None),
        P(("rep", "fs"), None),
        P(("rep", "fs"), None),
        P("fs", "tp"),
        P("fs", "tp"),
        P("fs", "tp"),
        P("fs", "tp"),
        P("fs", "tp"),
        P("fs", "tp"),
    )
    reps, shards, blocks = (mesh.shape[axis] for axis in ("rep", "fs", "tp"))

    def chosen(*arrays):
        rows = arrays[0].shape[0]
        depth, units = arrays[3].shape
        fits = (
            reps == 2
            and blocks == 2
            and shards % 2 == 0
            and units % (shards * 16) == 0
            and depth % 256 == 0
            and rows % 64 == 0
            and units % 256 == 0
            and arrays[0].shape[1] % 512 == 0
        )
        return split_hidden(shards, *arrays) if fits else per_device(*arrays)

    return jax.shard_map(
        chosen,
        mesh=mesh,
        in_specs=placed,
        out_specs=(
            P(("rep", "fs"), None),
            P(("rep", "fs"), None),
            P("fs", "tp"),
            P("fs", "tp"),
            P("fs", "tp"),
        ),
        check_vma=False,
    )
```

profile of v0, /device:TPU:12, one launch (start us, length us, event | category | flops | bytes accessed | tf_op | source)
XLA Modules:
  0.0 187.1 jit_solution(2397838190572277713)
XLA Ops:
  0.6 0.0 copy-start
  0.6 0.0 copy-start.1
  0.7 1.5 copy.14
  2.2 0.0 copy-done
  2.2 0.3 copy.15
  2.5 0.0 copy-done.1
  2.5 0.3 copy.16
  2.7 0.0 copy-start.4
  2.8 0.0 copy-start.5
  2.8 0.0 copy-start.6
  2.8 1.7 pad_maximum_fusion.wt
  4.5 0.0 copy-done.4
  4.5 0.0 copy-done.5
  4.5 0.1 copy-done.6
  4.5 1.3 pad_maximum_fusion.1.tok
  5.8 173.0 %fused.1 = (bf16[128,2048]{1,0:T(8,128)(2,1)}, bf16[128,2048]{1,0:T(8,128)(2,1)}, bf16[3,1536,256]{2,1,0:T(8,128)(2,1)}) custom-call(bf16[3,128,2048]{2,1,0:T(8,128)(2,1)} %pad_maximum_fusion.1.tok, bf16[3,1536,256]{2,1,0:T(8,128)(2,1)} %pad_maximum_fusion.wt), custom_call_target="tpu_custom_call" | custom-call | tf_op jit(solution)/shard_map/fused/pallas_call | solution.py:292
  178.8 0.0 copy-start.3
  178.9 0.0 copy-start.2
  178.9 6.6 %add_turned.1 = (f32[256,1536]{1,0:T(8,128)}, f32[256,1536]{1,0:T(8,128)}, f32[256,1536]{1,0:T(8,128)}) custom-call(bf16[3,1536,256]{2,1,0:T(8,128)(2,1)} %get-tuple-element.13.total, f32[256,1536]{1,0:T(8,128)} %first.1, f32[256,1536]{1,0:T(8,128)} %second.1, f32[256,1536]{1,0:T(8,128)} %third.1), custom_call_target="tpu_custom_call" | custom-call | tf_op jit(solution)/shard_map/add_turned/pallas_call | solution.py:256
  185.5 0.0 copy-done.3
  185.5 0.8 copy.19
  186.3 0.0 copy-done.2
  186.3 0.8 copy.20
Async XLA Ops:
  0.6 1.5 copy-start
  0.6 1.8 copy-start.1
  2.7 1.7 copy-start.4
  2.8 1.7 copy-start.5
  2.8 1.7 copy-start.6
  178.8 6.6 %copy-start.3 = (bf16[128,2048]{1,0:T(8,128)(2,1)S(1)}, bf16[128,2048]{1,0:T(8,128)(2,1)}, u32[]{:S(2)}) copy-start(bf16[128,2048]{1,0:T(8,128)(2,1)} %get-tuple-element.22) | copy-start | bytes 1572868
  178.9 7.4 %copy-start.2 = (bf16[128,2048]{1,0:T(8,128)(2,1)S(1)}, bf16[128,2048]{1,0:T(8,128)(2,1)}, u32[]{:S(2)}) copy-start(bf16[128,2048]{1,0:T(8,128)(2,1)} %get-tuple-element.23) | copy-start | bytes 1572868
where the time goes:
time: 187 us
  Pallas kernels  180 us (96%)
  local copies, waits for them, and re-layouts  3.73 us (2%)
  other arithmetic  2.99 us (2%)
    pallas_call x1, Pallas kernels, split_hidden(): pl.pallas_call(functools.partial(fused_kernel, n), out_shape=(jax.ShapeDt...  173 us
    pallas_call x1, Pallas kernels, add_turned(): pl.pallas_call(add_kernel, grid=(ff // width,), out_shape=tuple((jax.Shap...  6.6 us

commit v1 on v0

v1 whole, which is shorter than its diff:
```python
import functools

import jax
import jax.numpy as jnp
from jax import lax
from jax.experimental import pallas as pl
from jax.experimental.pallas import tpu as pltpu
from jax.sharding import PartitionSpec as P

MESH = pl.DeviceIdType.MESH


def flip(index, k, n):
    out, bit = 0, 1
    while bit < n:
        digit = lax.rem(index // bit, 2)
        out = out + bit * ((1 - digit) if k & bit else digit)
        bit *= 2
    return out


def span(start, size, step):
    return pl.ds(pl.multiple_of(start, step), size)


def remote(source, target, send, recv, device):
    return pltpu.make_async_remote_copy(
        src_ref=source,
        dst_ref=target,
        send_sem=send,
        recv_sem=recv,
        device_id=device,
        device_id_type=MESH,
    )


def fused_kernel(
    nz, later, earlier, cot, gw, uw, dw, late_out, early_out, g_out,
    slots, w, hid, part, peer, rin, rout, fin, gown, gyo, gyi, gxo, gxi, gzo,
    wzs, wzr, wxs, wxr, wys, wyr, aos, ags, agr, cs, cr,
    tds, tdr, rss, rsr, os_, or_, gys, gyr, gxs, gxr, gzs, gzr, gfs, gfr,
):
    r, f, t = lax.axis_index("rep"), lax.axis_index("fs"), lax.axis_index("tp")
    y, z = lax.rem(f, 2), f // 2
    m, width = later.shape
    q = m // 2
    dl, u = gw.shape[0], w.shape[2]
    hr = dl // 2
    f32, bf16 = jnp.float32, jnp.bfloat16
    outs = (late_out, early_out)
    to_x, to_y, to_t = {"rep": 1 - r}, {"fs": z * 2 + 1 - y}, {"tp": 1 - t}

    def layer(height):
        return {"fs": height * 2 + y}

    barrier = pltpu.get_barrier_semaphore()
    for device in [layer(flip(z, k, nz)) for k in range(1, nz)] + [to_x, to_y, to_t]:
        pl.semaphore_signal(barrier, inc=1, device_id=device, device_id_type=MESH)
    pl.semaphore_wait(barrier, nz + 2)

    pending = []

    def go(copy):
        copy.start()
        pending.append((None, copy))

    def when_go(condition, copy):
        @pl.when(condition)
        def _():
            copy.start()

        pending.append((condition, copy))

    def rows(side, height, h):
        return span((height * 2 + side) * dl + h * hr, hr, hr)

    def piece(side, height, h):
        return w.at[:, rows(side, height, h), :]

    def units(height):
        return span(height * u, u, u)

    def send_inputs(height, send, recv, device):
        for i, weight in enumerate((gw, uw, dw)):
            remote(weight.at[span(r * hr, hr, hr), units(height)], w.at[i, rows(y, z, r), :], send, recv, device).start()
        block = piece(y, z, r)
        pending.append((None, remote(block, block, send, recv, device)))

    def wx(k, a, block):
        return remote(block, block, wxs.at[k, a], wxr.at[k, a], to_x)

    def wy(k, a, block):
        return remote(block, block, wys.at[k, a], wyr.at[k, a], to_y)

    def spread(k):
        block = piece(y, flip(z, k, nz), r)
        remote(block, block, wzs.at[k], wzr.at[k], to_x).wait_recv()
        go(wx(k, 0, block))
        go(wy(k, 0, block))

    def relay(k):
        height = flip(z, k, nz)
        if k % 2:
            block = piece(y, height, 1 - r)
            wx(k, 0, block).wait_recv()
            go(wy(k, 1, block))
        else:
            block = piece(1 - y, height, r)
            wy(k, 0, block).wait_recv()
            go(wx(k, 1, block))

    def gathered(k):
        height = flip(z, k, nz)
        if k % 2:
            wy(k, 0, piece(1 - y, height, r)).wait_recv()
            wy(k, 1, piece(1 - y, height, 1 - r)).wait_recv()
        else:
            if k:
                wx(k, 0, piece(y, height, 1 - r)).wait_recv()
            wx(k, 1, piece(1 - y, height, 1 - r)).wait_recv()

    arrays = (pl.ds(1, 2), pl.ds(0, 1))

    def half(core):
        return span(core * q, q, q)

    def block_of(g, origin, core):
        return slots.at[arrays[g], origin, half(core), :]

    def step_of(d):
        return 1 - 2 * d

    def exists(height):
        return jnp.logical_and(height >= 0, height < nz)

    def send_own(g):
        for d in range(2):
            device = layer(z + step_of(d))
            sources = ((1, earlier), (2, cot)) if g == 0 else ((0, later),)

            @pl.when(exists(z + step_of(d)))
            def _():
                for i, source in sources:
                    remote(
                        source.at[half(t), :], slots.at[i, z, half(t), :], aos.at[g, d], agr.at[g, z], device
                    ).start()

            block = block_of(g, z, t)
            pending.append((exists(z + step_of(d)), remote(block, block, aos.at[g, d], agr.at[g, z], device)))

    def take_on(g, k):
        for d in range(2):
            origin, target = z - step_of(d) * k, z + step_of(d)
            block = block_of(g, origin, t)
            ahead = remote(block, block, ags.at[g, k, d], agr.at[g, origin], layer(target))
            over = remote(block, block, cs.at[g, k, d], cr.at[g, k, d], to_t)

            @pl.when(exists(origin))
            def _():
                ahead.wait_recv()

            when_go(jnp.logical_and(exists(origin), exists(target)), ahead)
            when_go(exists(origin), over)

    def whole(g, k, d):
        block = block_of(g, z - step_of(d) * k, 1 - t)
        remote(block, block, cs.at[g, k, d], cr.at[g, k, d], to_t).wait_recv()

    def each_block(g, k, body):
        if k == 0:
            body(z)
            return
        for d in range(2):
            @pl.when(exists(z - step_of(d) * k))
            def _():
                whole(g, k, d)

        def one(d, carry):
            origin = z - step_of(d) * k

            @pl.when(exists(origin))
            def _():
                body(origin)

            return carry

        lax.fori_loop(0, 2, one, 0)

    def early(b):
        gate = jnp.dot(slots[1, b], w[0], preferred_element_type=f32)
        up = jnp.dot(slots[1, b], w[1], preferred_element_type=f32)
        hidden_grad = jnp.dot(slots[2, b], w[2], preferred_element_type=f32)
        hid[0, b], hid[1, b], hid[2, b] = early_parts(gate, up, hidden_grad)

    step = width // 4

    def trade(o, b):
        return remote(part.at[o, b, half(1 - t), :], peer.at[o, b], tds.at[o, b], tdr.at[o, b], to_t)

    def late(b):
        gate = jnp.dot(slots[0, b], w[0], preferred_element_type=f32)
        up = jnp.dot(slots[0, b], w[1], preferred_element_type=f32)
        hidden = (jax.nn.silu(gate) * up).astype(bf16)
        for c in range(4):
            lanes = slice(c * step, (c + 1) * step)
            part[0, b, :, lanes] = contract_last(hidden, w[2, lanes, :]).astype(bf16)
        trade(0, b).start()

    def input_grad(b, carry):
        for c in range(4):
            lanes = slice(c * step, (c + 1) * step)
            part[1, b, :, lanes] = (
                contract_last(hid[0, b], w[0, lanes, :]) + contract_last(hid[1, b], w[1, lanes, :])
            ).astype(bf16)
        trade(1, b).start()
        return carry

    def own(o, b):
        return part[o, b, half(t), :].astype(f32) + peer[o, b].astype(f32)

    def traded(o, b):
        remote(peer.at[o, b], peer.at[o, b], tds.at[o, b], tdr.at[o, b], to_t).wait_recv()

    def sum_copy(o, d, b):
        return remote(rout.at[o, b], rin.at[d, o, b], rss.at[o, b], rsr.at[d, o, b], layer(z + step_of(d)))

    def sum_pass(o, p):
        for d in range(2):
            @pl.when(z == (nz - 1 - p if d else p))
            def _():
                def one(i, carry):
                    b = i if d else nz - 1 - i
                    traded(o, b)
                    value = own(o, b)
                    if p:
                        slot = rin.at[d, o, b]
                        remote(slot, slot, rss.at[o, b], rsr.at[d, o, b], to_t).wait_recv()
                        value = value + rin[d, o, b].astype(f32)
                    rout[o, b] = value.astype(bf16)
                    sum_copy(o, d, b).start()
                    return carry

                lax.fori_loop(0, nz - 1 - p, one, 0)

    def sum_end(o):
        traded(o, z)
        fin[...] = own(o, z)
        for d in range(2):
            @pl.when(exists(z - step_of(d)))
            def _():
                slot = rin.at[d, o, z]
                remote(slot, slot, rss.at[o, z], rsr.at[d, o, z], to_t).wait_recv()
                fin[...] += rin[d, o, z].astype(f32)

        outs[o][half(t), :] = fin[...].astype(bf16)
        mine = outs[o].at[half(t), :]
        go(remote(mine, mine, os_.at[o], or_.at[o], to_t))

    def grad_block(side, height, i):
        lanes = span((height * 2 + side) * dl, dl, dl)
        source = slots[2 if i == 2 else 1, :, :, lanes].reshape(nz * m, dl)
        return contract_first(source, hid[i].reshape(nz * m, u))

    def grad_send(k):
        for i in range(3):
            gyo[k, i] = grad_block(1 - y, flip(z, k, nz), i).astype(bf16)
        go(remote(gyo.at[k], gyi.at[k], gys.at[k], gyr.at[k], to_y))

    def grad_own(k):
        for i in range(3):
            gown[k, i] = grad_block(y, flip(z, k, nz), i)

    def grad_x(k):
        remote(gyi.at[k], gyi.at[k], gys.at[k], gyr.at[k], to_y).wait_recv()
        theirs = span((1 - r) * hr, hr, hr)
        gxo[k] = (gown[k, :, theirs, :] + gyi[k, :, theirs, :].astype(f32)).astype(bf16)
        go(remote(gxo.at[k], gxi.at[k], gxs.at[k], gxr.at[k], to_x))

    def g_block(height, h):
        return g_out.at[:, span(h * hr, hr, hr), units(height)]

    def grad_z(k):
        remote(gxi.at[k], gxi.at[k], gxs.at[k], gxr.at[k], to_x).wait_recv()
        mine = span(r * hr, hr, hr)
        total = (
            gown[k, :, mine, :] + gyi[k, :, mine, :].astype(f32) + gxi[k].astype(f32)
        ).astype(bf16)
        if k:
            gzo[k] = total
            go(remote(gzo.at[k], g_block(z, r), gzs.at[k], gzr.at[k], layer(flip(z, k, nz))))
        else:
            g_out[:, mine, units(z)] = total

    def g_copy(k, h):
        block = g_block(flip(z, k, nz), h)
        return remote(block, block, gfs.at[k], gfr.at[k], to_x)

    def grad_x_back(k):
        if k:
            block = g_block(flip(z, k, nz), r)
            remote(block, block, gzs.at[k], gzr.at[k], to_x).wait_recv()
        go(g_copy(k, r))

    for k in range(1, nz):
        send_inputs(flip(z, k, nz), wzs.at[k], wzr.at[k], layer(flip(z, k, nz)))
    send_inputs(z, wys.at[0, 0], wyr.at[0, 0], to_y)
    send_own(0)
    slots[0, z] = later[...]
    slots[1, z] = earlier[...]
    slots[2, z] = cot[...]
    for i, weight in enumerate((gw, uw, dw)):
        w[i, span((z * 2 + y) * dl, dl, dl), :] = weight[:, units(z)]
    relay(0)
    for k in range(1, nz):
        spread(k)
        if k > 1:
            relay(k - 1)
    relay(nz - 1)
    take_on(0, 1)
    for k in range(nz):
        gathered(k)
    for k in range(nz):
        each_block(0, k, early)
        if k + 2 < nz:
            take_on(0, k + 2)
        if k == max(nz - 4, 0):
            send_own(1)
    take_on(1, 1)
    order = list(range(nz - 1, -1, -1))
    for k in order:
        grad_send(k)
    for k in range(2, nz):
        take_on(1, k)
    for k in order:
        grad_own(k)
    lax.fori_loop(0, nz, input_grad, 0)

    tasks = []
    for i in range(nz + 2):
        chain = []
        if i >= 2:
            chain.append((grad_x_back, order[i - 2]))
        if 1 <= i <= nz:
            chain.append((grad_z, order[i - 1]))
        if i < nz:
            chain.append((grad_x, order[i]))
        tasks.append(chain)
    for i in range(nz + 2):
        for task, k in tasks[i]:
            task(k)
        if i < nz:
            each_block(1, i, late)
        if i < nz - 1:
            sum_pass(1, i)
        if i == nz - 1:
            sum_end(1)
        if i >= 2 and i - 2 < nz - 1:
            pass
        if i == nz - 1:
            for p in range(nz - 1):
                sum_pass(0, p)
        if i == nz:
            sum_end(0)
    for k in range(nz):
        g_copy(k, 1 - r).wait_recv()
    for o in range(2):
        other = outs[o].at[half(1 - t), :]
        remote(other, other, os_.at[o], or_.at[o], to_t).wait_recv()
    for o in range(2):
        for b in range(nz):
            trade(o, b).wait_send()

            @pl.when(z != b)
            def _():
                sum_copy(o, 0, b).wait_send()

    for condition, copy in pending:
        if condition is None:
            copy.wait_send()
        else:
            @pl.when(condition)
            def _():
                copy.wait_send()


VMEM = pl.BlockSpec(memory_space=pltpu.VMEM)


def dma(*shape):
    return pltpu.SemaphoreType.DMA(shape)


def split_hidden(
    n,
    later_input,
    earlier_input,
    cotangent,
    gate_weight,
    up_weight,
    down_weight,
    gate_sum,
    up_sum,
    down_sum,
):
    bf16, f32 = jnp.bfloat16, jnp.float32
    m, width = later_input.shape
    dl, ff = gate_weight.shape
    nz = n // 2
    u, q, hr = ff // nz, m // 2, dl // 2
    later_output, earlier_input_grad, total = pl.pallas_call(
        functools.partial(fused_kernel, nz),
        out_shape=(
            jax.ShapeDtypeStruct((m, width), bf16),
            jax.ShapeDtypeStruct((m, width), bf16),
            jax.ShapeDtypeStruct((3, dl, ff), bf16),
        ),
        in_specs=[VMEM] * 6,
        out_specs=(VMEM, VMEM, VMEM),
        scratch_shapes=[
            pltpu.VMEM((3, nz, m, width), bf16),
            pltpu.VMEM((3, width, u), bf16),
            pltpu.VMEM((3, nz, m, u), bf16),
            pltpu.VMEM((2, nz, m, width), bf16),
            pltpu.VMEM((2, nz, q, width), bf16),
            pltpu.VMEM((2, 2, nz, q, width), bf16),
            pltpu.VMEM((2, nz, q, width), bf16),
            pltpu.VMEM((q, width), f32),
            pltpu.VMEM((nz, 3, dl, u), f32),
            pltpu.VMEM((nz, 3, dl, u), bf16),
            pltpu.VMEM((nz, 3, dl, u), bf16),
            pltpu.VMEM((nz, 3, hr, u), bf16),
            pltpu.VMEM((nz, 3, hr, u), bf16),
            pltpu.VMEM((nz, 3, hr, u), bf16),
        ]
        + [dma(nz)] * 2
        + [dma(nz, 2)] * 4
        + [dma(2, 2), dma(2, nz, 2), dma(2, nz), dma(2, nz, 2), dma(2, nz, 2)]
        + [dma(2, nz), dma(2, nz), dma(2, nz), dma(2, 2, nz), dma(2), dma(2)]
        + [dma(nz)] * 8,
        compiler_params=pltpu.CompilerParams(
            collective_id=0, has_side_effects=True, vmem_limit_bytes=50 * 2**20
        ),
        name="fused",
    )(later_input, earlier_input, cotangent, gate_weight, up_weight, down_weight)
    sums = tuple(old + total[i].astype(f32) for i, old in enumerate((gate_sum, up_sum, down_sum)))
    return (later_output, earlier_input_grad) + sums


def early_parts(gate_early, up_early, hidden_grad):
    sigmoid_gate = jax.nn.sigmoid(gate_early)
    silu_early = gate_early * sigmoid_gate
    gate_grad = (
        hidden_grad * up_early * sigmoid_gate * (1.0 + gate_early * (1.0 - sigmoid_gate))
    ).astype(jnp.bfloat16)
    up_grad = (hidden_grad * silu_early).astype(jnp.bfloat16)
    hidden_early = (silu_early * up_early).astype(jnp.bfloat16)
    return gate_grad, up_grad, hidden_early


def contract_last(first, second):
    return lax.dot_general(
        first, second, (((1,), (1,)), ((), ())), preferred_element_type=jnp.float32
    )


def contract_first(first, second):
    return lax.dot_general(
        first, second, (((0,), (0,)), ((), ())), preferred_element_type=jnp.float32
    )


def per_device(
    later_input,
    earlier_input,
    cotangent,
    gate_weight,
    up_weight,
    down_weight,
    gate_sum,
    up_sum,
    down_sum,
):
    gate_full, up_full, down_full = (
        lax.all_gather(gate_weight, "fs", axis=0, tiled=True),
        lax.all_gather(up_weight, "fs", axis=0, tiled=True),
        lax.all_gather(down_weight, "fs", axis=0, tiled=True),
    )
    gate_late = jnp.dot(later_input, gate_full, preferred_element_type=jnp.float32)
    up_late = jnp.dot(later_input, up_full, preferred_element_type=jnp.float32)
    hidden_late = (jax.nn.silu(gate_late) * up_late).astype(jnp.bfloat16)
    partial_late = contract_last(hidden_late, down_full)
    later_output = lax.psum(partial_late.astype(jnp.bfloat16), "tp")
    gate_early = jnp.dot(earlier_input, gate_full, preferred_element_type=jnp.float32)
    up_early = jnp.dot(earlier_input, up_full, preferred_element_type=jnp.float32)
    hidden_grad = jnp.dot(cotangent, down_full, preferred_element_type=jnp.float32)
    sigmoid_gate = jax.nn.sigmoid(gate_early)
    silu_early = gate_early * sigmoid_gate
    gate_grad = (
        hidden_grad * up_early * sigmoid_gate * (1.0 + gate_early * (1.0 - sigmoid_gate))
    ).astype(jnp.bfloat16)
    up_grad = (hidden_grad * silu_early).astype(jnp.bfloat16)
    hidden_early = (silu_early * up_early).astype(jnp.bfloat16)
    partial_early = contract_last(gate_grad, gate_full) + contract_last(up_grad, up_full)
    earlier_input_grad = lax.psum(partial_early.astype(jnp.bfloat16), "tp")
    columns, cot_columns = (
        lax.all_to_all(earlier_input, "fs", split_axis=1, concat_axis=0, tiled=True),
        lax.all_to_all(cotangent, "fs", split_axis=1, concat_axis=0, tiled=True),
    )
    gate_local = contract_first(columns, lax.all_gather(gate_grad, "fs", axis=0, tiled=True))
    up_local = contract_first(columns, lax.all_gather(up_grad, "fs", axis=0, tiled=True))
    down_local = contract_first(cot_columns, lax.all_gather(hidden_early, "fs", axis=0, tiled=True))
    gate_total, up_total, down_total = (
        lax.psum(gate_local.astype(jnp.bfloat16), "rep").astype(jnp.float32),
        lax.psum(up_local.astype(jnp.bfloat16), "rep").astype(jnp.float32),
        lax.psum(down_local.astype(jnp.bfloat16), "rep").astype(jnp.float32),
    )
    return (
        later_output,
        earlier_input_grad,
        gate_sum + gate_total,
        up_sum + up_total,
        down_sum + down_total,
    )


def solution(mesh):
    placed = (
        P(("rep", "fs"), None),
        P(("rep", "fs"), None),
        P(("rep", "fs"), None),
        P("fs", "tp"),
        P("fs", "tp"),
        P("fs", "tp"),
        P("fs", "tp"),
        P("fs", "tp"),
        P("fs", "tp"),
    )
    reps, shards, blocks = (mesh.shape[axis] for axis in ("rep", "fs", "tp"))

    def chosen(*arrays):
        rows = arrays[0].shape[0]
        depth, units = arrays[3].shape
        layers = shards // 2
        fits = (
            reps == 2
            and blocks == 2
            and layers >= 2
            and shards == 2 * layers
            and layers & (layers - 1) == 0
            and units % (layers * 128) == 0
            and depth % 128 == 0
            and rows % 32 == 0
            and arrays[0].shape[1] % 512 == 0
            and arrays[0].shape[1] == depth * shards
        )
        return split_hidden(shards, *arrays) if fits else per_device(*arrays)

    return jax.shard_map(
        chosen,
        mesh=mesh,
        in_specs=placed,
        out_specs=(
            P(("rep", "fs"), None),
            P(("rep", "fs"), None),
            P("fs", "tp"),
            P("fs", "tp"),
            P("fs", "tp"),
        ),
        check_vma=False,
    )
```

time: 187 us -> 176 us (0.941)
  the two profiles are of different devices: /device:TPU:12 before, /device:TPU:0 now
where the time goes in v1:
time: 176 us
  Pallas kernels  165 us (94%)
  local copies, waits for them, and re-layouts  5.84 us (3%)
  other arithmetic  4.5 us (3%)
    pallas_call x1, Pallas kernels, split_hidden(): pl.pallas_call(functools.partial(fused_kernel, nz), out_shape=(jax.ShapeD...  165 us
    unnamed x14, local copies, waits for them, and re-layouts  5.84 us
    add x1, other arithmetic, split_hidden(): old + total[i].astype(f32)  4.5 us

profile of v1, /device:TPU:0, one launch (start us, length us, event | category | flops | bytes accessed | tf_op | source)
XLA Modules:
  0.0 176.0 jit_solution(5419929563600808103)
XLA Ops:
  0.6 0.0 copy-start
  0.6 1.1 copy-done
  1.8 0.0 copy-start.1
  1.8 1.0 copy-done.1
  2.8 0.0 copy-start.2
  2.8 1.0 copy-done.2
  3.9 0.0 copy-start.3
  3.9 1.0 copy-done.3
  4.9 0.0 copy-start.4
  4.9 0.0 copy-start.5
  4.9 165.0 %fused.1 = (bf16[128,2048]{1,0:T(8,128)(2,1)S(1)}, bf16[128,2048]{1,0:T(8,128)(2,1)S(1)}, bf16[3,256,1536]{2,1,0:T(8,128)(2,1)}) custom-call(bf16[128,2048]{1,0:T(8,128)(2,1)S(1)} %copy-done.1, bf16[128,2048]{1,0:T(8,128)(2,1)S(1)} %copy-done.2, bf16[128,2048]{1,0:T(8,128)(2,1)S(1)} %copy-done.3, bf16[256,1536]{1,0:T(8,128)(2,1)S(1)} %copy-done, ...), custom_call_target="tpu_custom_call" | custom-call | tf_op jit(solution)/shard_map/fused/pallas_call | solution.py:410
  169.9 0.0 copy-done.4
  169.9 0.0 copy-done.5
  169.9 4.5 %convert_add_fusion = (f32[256,1536]{1,0:T(8,128)}, f32[256,1536]{1,0:T(8,128)}, f32[256,1536]{1,0:T(8,128)}) fusion(f32[256,1536]{1,0:T(8,128)S(1)} %copy-done.4, bf16[3,256,1536]{2,1,0:T(8,128)(2,1)} %get-tuple-element.10, f32[256,1536]{1,0:T(8,128)S(1)} %copy-done.5, f32[256,1536]{1,0:T(8,128)} %param.15), kind=kLoop, calls=%fused_computation | loop fusion | flops 2359296 | bytes 11796480 | tf_op jit(solution)/shard_map/add | solution.py:445
  174.4 0.8 copy.16
  175.2 0.8 copy.17
Async XLA Ops:
  0.6 1.1 copy-start
  1.8 1.0 copy-start.1
  2.8 1.0 copy-start.2
  3.9 1.0 copy-start.3
  4.9 165.0 %copy-start.4 = (f32[256,1536]{1,0:T(8,128)S(1)}, f32[256,1536]{1,0:T(8,128)}, u32[]{:S(2)}) copy-start(f32[256,1536]{1,0:T(8,128)} %param.17) | copy-start | bytes 4718596
  4.9 165.0 %copy-start.5 = (f32[256,1536]{1,0:T(8,128)S(1)}, f32[256,1536]{1,0:T(8,128)}, u32[]{:S(2)}) copy-start(f32[256,1536]{1,0:T(8,128)} %param.16) | copy-start | bytes 4718596

commit v2 on v1

--- a/solution.py
+++ b/solution.py
@@ -34,10 +34,13 @@
     )
 
 
+EARLY, COT, LATE = 0, 1, 2
+
+
 def fused_kernel(
-    nz, later, earlier, cot, gw, uw, dw, late_out, early_out, g_out,
-    slots, w, hid, part, peer, rin, rout, fin, gown, gyo, gyi, gxo, gxi, gzo,
-    wzs, wzr, wxs, wxr, wys, wyr, aos, ags, agr, cs, cr,
+    nz, later, earlier, cot, gw, uw, dw, gsum, usum, dsum, late_out, early_out, gnew, unew, dnew,
+    slots, wt, w, g_out, hid, part, peer, rin, rout, gown, gyo, gyi, gxo, gxi, gzo,
+    lts, lws, los, lns, wzs, wzr, wxs, wxr, wys, wyr, aos, ags, agr, cs, cr,
     tds, tdr, rss, rsr, os_, or_, gys, gyr, gxs, gxr, gzs, gzr, gfs, gfr,
 ):
     r, f, t = lax.axis_index("rep"), lax.axis_index("fs"), lax.axis_index("tp")
@@ -53,6 +56,24 @@
     def layer(height):
         return {"fs": height * 2 + y}
 
+    def units(height):
+        return span(height * u, u, u)
+
+    slot_of = (1, 2, 0)
+    local_tokens = [
+        pltpu.make_async_copy(source, slots.at[slot_of[g], z], lts.at[g])
+        for g, source in enumerate((earlier, cot, later))
+    ]
+    local_weights = [pltpu.make_async_copy(source, wt.at[i], lws.at[i]) for i, source in enumerate((gw, uw, dw))]
+    local_own = [
+        pltpu.make_async_copy(source.at[:, units(z)], w.at[i, span((z * 2 + y) * dl, dl, dl), :], los.at[i])
+        for i, source in enumerate((gw, uw, dw))
+    ]
+    news = (gnew, unew, dnew)
+    local_sums = [pltpu.make_async_copy(source, news[i], lns.at[i]) for i, source in enumerate((gsum, usum, dsum))]
+    for copy in local_weights + local_tokens + local_own + local_sums:
+        copy.start()
+
     barrier = pltpu.get_barrier_semaphore()
     for device in [layer(flip(z, k, nz)) for k in range(1, nz)] + [to_x, to_y, to_t]:
         pl.semaphore_signal(barrier, inc=1, device_id=device, device_id_type=MESH)
@@ -77,14 +98,8 @@
     def piece(side, height, h):
         return w.at[:, rows(side, height, h), :]
 
-    def units(height):
-        return span(height * u, u, u)
-
-    def send_inputs(height, send, recv, device):
-        for i, weight in enumerate((gw, uw, dw)):
-            remote(weight.at[span(r * hr, hr, hr), units(height)], w.at[i, rows(y, z, r), :], send, recv, device).start()
-        block = piece(y, z, r)
-        pending.append((None, remote(block, block, send, recv, device)))
+    def send_weights(height, send, recv, device):
+        go(remote(wt.at[:, span(r * hr, hr, hr), units(height)], piece(y, z, r), send, recv, device))
 
     def wx(k, a, block):
         return remote(block, block, wxs.at[k, a], wxr.at[k, a], to_x)
@@ -119,13 +134,11 @@
                 wx(k, 0, piece(y, height, 1 - r)).wait_recv()
             wx(k, 1, piece(1 - y, height, 1 - r)).wait_recv()
 
-    arrays = (pl.ds(1, 2), pl.ds(0, 1))
-
     def half(core):
         return span(core * q, q, q)
 
     def block_of(g, origin, core):
-        return slots.at[arrays[g], origin, half(core), :]
+        return slots.at[slot_of[g], origin, half(core), :]
 
     def step_of(d):
         return 1 - 2 * d
@@ -135,18 +148,9 @@
 
     def send_own(g):
         for d in range(2):
-            device = layer(z + step_of(d))
-            sources = ((1, earlier), (2, cot)) if g == 0 else ((0, later),)
-
-            @pl.when(exists(z + step_of(d)))
-            def _():
-                for i, source in sources:
-                    remote(
-                        source.at[half(t), :], slots.at[i, z, half(t), :], aos.at[g, d], agr.at[g, z], device
-                    ).start()
-
+            target = z + step_of(d)
             block = block_of(g, z, t)
-            pending.append((exists(z + step_of(d)), remote(block, block, aos.at[g, d], agr.at[g, z], device)))
+            when_go(exists(target), remote(block, block, aos.at[g, d], agr.at[g, z], layer(target)))
 
     def take_on(g, k):
         for d in range(2):
@@ -162,21 +166,21 @@
             when_go(jnp.logical_and(exists(origin), exists(target)), ahead)
             when_go(exists(origin), over)
 
-    def whole(g, k, d):
-        block = block_of(g, z - step_of(d) * k, 1 - t)
-        remote(block, block, cs.at[g, k, d], cr.at[g, k, d], to_t).wait_recv()
-
-    def each_block(g, k, body):
+    def whole(g, k):
+        for d in range(2):
+            block = block_of(g, z - step_of(d) * k, 1 - t)
+
+            @pl.when(exists(z - step_of(d) * k))
+            def _():
+                remote(block, block, cs.at[g, k, d], cr.at[g, k, d], to_t).wait_recv()
+
+    def each_block(k, body):
         if k == 0:
             body(z)
             return
-        for d in range(2):
-            @pl.when(exists(z - step_of(d) * k))
-            def _():
-                whole(g, k, d)
 
         def one(d, carry):
-            origin = z - step_of(d) * k
+            origin = z - (1 - 2 * d) * k
 
             @pl.when(exists(origin))
             def _():
@@ -191,6 +195,12 @@
         up = jnp.dot(slots[1, b], w[1], preferred_element_type=f32)
         hidden_grad = jnp.dot(slots[2, b], w[2], preferred_element_type=f32)
         hid[0, b], hid[1, b], hid[2, b] = early_parts(gate, up, hidden_grad)
+
+    def early_level(k):
+        if k:
+            whole(EARLY, k)
+            whole(COT, k)
+        each_block(k, early)
 
     step = width // 4
 
@@ -206,53 +216,78 @@
             part[0, b, :, lanes] = contract_last(hidden, w[2, lanes, :]).astype(bf16)
         trade(0, b).start()
 
-    def input_grad(b, carry):
+    def late_level(k):
+        if k:
+            whole(LATE, k)
+        each_block(k, late)
+
+    def input_grad(b):
         for c in range(4):
             lanes = slice(c * step, (c + 1) * step)
             part[1, b, :, lanes] = (
                 contract_last(hid[0, b], w[0, lanes, :]) + contract_last(hid[1, b], w[1, lanes, :])
             ).astype(bf16)
         trade(1, b).start()
-        return carry
-
-    def own(o, b):
-        return part[o, b, half(t), :].astype(f32) + peer[o, b].astype(f32)
+
+    fine = 16
 
     def traded(o, b):
         remote(peer.at[o, b], peer.at[o, b], tds.at[o, b], tdr.at[o, b], to_t).wait_recv()
 
-    def sum_copy(o, d, b):
-        return remote(rout.at[o, b], rin.at[d, o, b], rss.at[o, b], rsr.at[d, o, b], layer(z + step_of(d)))
-
-    def sum_pass(o, p):
-        for d in range(2):
-            @pl.when(z == (nz - 1 - p if d else p))
-            def _():
-                def one(i, carry):
-                    b = i if d else nz - 1 - i
-                    traded(o, b)
-                    value = own(o, b)
-                    if p:
-                        slot = rin.at[d, o, b]
-                        remote(slot, slot, rss.at[o, b], rsr.at[d, o, b], to_t).wait_recv()
-                        value = value + rin[d, o, b].astype(f32)
-                    rout[o, b] = value.astype(bf16)
-                    sum_copy(o, d, b).start()
-                    return carry
-
-                lax.fori_loop(0, nz - 1 - p, one, 0)
+    def chunks(body):
+        def one(i, carry):
+            body(i * fine)
+            return carry
+
+        lax.fori_loop(0, q // fine, one, 0)
+
+    def own(o, b, start):
+        return (
+            part[o, b, span(t * q + start, fine, fine), :].astype(f32)
+            + peer[o, b, span(start, fine, fine), :].astype(f32)
+        )
+
+    def sum_copy(o, d, b, device):
+        return remote(rout.at[o, b], rin.at[d, o, b], rss.at[o, b], rsr.at[d, o, b], device)
+
+    def sum_step(o, far, h):
+        @pl.when(jnp.logical_or(z == h, z == nz - 1 - h))
+        def _():
+            up = jnp.where(z == h, 1, 0)
+            d = 1 - up
+            b = up * far + d * (nz - 1 - far)
+            copy = sum_copy(o, d, b, layer(z + 2 * up - 1))
+            traded(o, b)
+            if h:
+                copy.wait_recv()
+
+            def add(start):
+                piece_rows = span(start, fine, fine)
+                value = own(o, b, start)
+                if h:
+                    value = value + rin[d, o, b, piece_rows, :].astype(f32)
+                rout[o, b, piece_rows, :] = value.astype(bf16)
+
+            chunks(add)
+            copy.start()
 
     def sum_end(o):
         traded(o, z)
-        fin[...] = own(o, z)
         for d in range(2):
             @pl.when(exists(z - step_of(d)))
             def _():
-                slot = rin.at[d, o, z]
-                remote(slot, slot, rss.at[o, z], rsr.at[d, o, z], to_t).wait_recv()
-                fin[...] += rin[d, o, z].astype(f32)
-
-        outs[o][half(t), :] = fin[...].astype(bf16)
+                sum_copy(o, d, z, to_t).wait_recv()
+
+        def add(start):
+            piece_rows = span(start, fine, fine)
+            value = own(o, z, start)
+            for d in range(2):
+                value = value + jnp.where(
+                    exists(z - step_of(d)), rin[d, o, z, piece_rows, :].astype(f32), 0.0
+                )
+            outs[o][span(t * q + start, fine, fine), :] = value.astype(bf16)
+
+        chunks(add)
         mine = outs[o].at[half(t), :]
         go(remote(mine, mine, os_.at[o], or_.at[o], to_t))
 
@@ -261,108 +296,165 @@
         source = slots[2 if i == 2 else 1, :, :, lanes].reshape(nz * m, dl)
         return contract_first(source, hid[i].reshape(nz * m, u))
 
-    def grad_send(k):
-        for i in range(3):
-            gyo[k, i] = grad_block(1 - y, flip(z, k, nz), i).astype(bf16)
-        go(remote(gyo.at[k], gyi.at[k], gys.at[k], gyr.at[k], to_y))
-
-    def grad_own(k):
-        for i in range(3):
-            gown[k, i] = grad_block(y, flip(z, k, nz), i)
-
-    def grad_x(k):
-        remote(gyi.at[k], gyi.at[k], gys.at[k], gyr.at[k], to_y).wait_recv()
-        theirs = span((1 - r) * hr, hr, hr)
-        gxo[k] = (gown[k, :, theirs, :] + gyi[k, :, theirs, :].astype(f32)).astype(bf16)
-        go(remote(gxo.at[k], gxi.at[k], gxs.at[k], gxr.at[k], to_x))
-
-    def g_block(height, h):
-        return g_out.at[:, span(h * hr, hr, hr), units(height)]
-
-    def grad_z(k):
-        remote(gxi.at[k], gxi.at[k], gxs.at[k], gxr.at[k], to_x).wait_recv()
-        mine = span(r * hr, hr, hr)
+    def grad_send(k, i):
+        gyo[k, i] = grad_block(1 - y, flip(z, k, nz), i).astype(bf16)
+        go(remote(gyo.at[k, i], gyi.at[k, i], gys.at[k, i], gyr.at[k, i], to_y))
+
+    def grad_own(k, i):
+        gown[k, i] = grad_block(y, flip(z, k, nz), i)
+
+    mine_rows, their_rows = span(r * hr, hr, hr), span((1 - r) * hr, hr, hr)
+
+    def grad_x(k, i):
+        remote(gyi.at[k, i], gyi.at[k, i], gys.at[k, i], gyr.at[k, i], to_y).wait_recv()
+        gxo[k, i] = (gown[k, i, their_rows, :] + gyi[k, i, their_rows, :].astype(f32)).astype(bf16)
+        go(remote(gxo.at[k, i], gxi.at[k, i], gxs.at[k, i], gxr.at[k, i], to_x))
+
+    def g_block(i, height, h):
+        return g_out.at[i, span(h * hr, hr, hr), units(height)]
+
+    def grad_z(k, i):
+        remote(gxi.at[k, i], gxi.at[k, i], gxs.at[k, i], gxr.at[k, i], to_x).wait_recv()
         total = (
-            gown[k, :, mine, :] + gyi[k, :, mine, :].astype(f32) + gxi[k].astype(f32)
+            gown[k, i, mine_rows, :] + gyi[k, i, mine_rows, :].astype(f32) + gxi[k, i].astype(f32)
         ).astype(bf16)
         if k:
-            gzo[k] = total
-            go(remote(gzo.at[k], g_block(z, r), gzs.at[k], gzr.at[k], layer(flip(z, k, nz))))
+            gzo[k, i] = total
+            go(remote(gzo.at[k, i], g_block(i, z, r), gzs.at[k, i], gzr.at[k, i], layer(flip(z, k, nz))))
         else:
-            g_out[:, mine, units(z)] = total
-
-    def g_copy(k, h):
-        block = g_block(flip(z, k, nz), h)
-        return remote(block, block, gfs.at[k], gfr.at[k], to_x)
-
-    def grad_x_back(k):
+            g_out[i, mine_rows, units(z)] = total
+
+    def g_copy(k, i, h):
+        block = g_block(i, flip(z, k, nz), h)
+        return remote(block, block, gfs.at[k, i], gfr.at[k, i], to_x)
+
+    def grad_back(k, i):
         if k:
-            block = g_block(flip(z, k, nz), r)
-            remote(block, block, gzs.at[k], gzr.at[k], to_x).wait_recv()
-        go(g_copy(k, r))
-
+            block = g_block(i, flip(z, k, nz), r)
+            remote(block, block, gzs.at[k, i], gzr.at[k, i], to_x).wait_recv()
+        go(g_copy(k, i, r))
+        grad_add(k, i, r)
+
+    def grad_add(k, i, h):
+        place = (span(h * hr, hr, hr), units(flip(z, k, nz)))
+        news[i][place] += g_out[(i,) + place].astype(f32)
+
+    def grad_last(k, i):
+        g_copy(k, i, 1 - r).wait_recv()
+        grad_add(k, i, 1 - r)
+
+    def run(name, task, *args):
+        with jax.named_scope(name + "_".join(str(a) for a in args if isinstance(a, int))):
+            task(*args)
+
+    def send_first():
+        for copy in local_weights:
+            copy.wait()
+        for k in range(1, nz):
+            send_weights(flip(z, k, nz), wzs.at[k], wzr.at[k], layer(flip(z, k, nz)))
+        send_weights(z, wys.at[0, 0], wyr.at[0, 0], to_y)
+        for copy in local_tokens:
+            copy.wait()
+        send_own(EARLY)
+        send_own(COT)
+        for copy in local_own:
+            copy.wait()
+
+    last = nz - 1
+    run("send_first", send_first)
+    run("relay", relay, 0)
     for k in range(1, nz):
-        send_inputs(flip(z, k, nz), wzs.at[k], wzr.at[k], layer(flip(z, k, nz)))
-    send_inputs(z, wys.at[0, 0], wyr.at[0, 0], to_y)
-    send_own(0)
-    slots[0, z] = later[...]
-    slots[1, z] = earlier[...]
-    slots[2, z] = cot[...]
-    for i, weight in enumerate((gw, uw, dw)):
-        w[i, span((z * 2 + y) * dl, dl, dl), :] = weight[:, units(z)]
-    relay(0)
-    for k in range(1, nz):
-        spread(k)
+        run("spread", spread, k)
         if k > 1:
-            relay(k - 1)
-    relay(nz - 1)
-    take_on(0, 1)
-    for k in range(nz):
-        gathered(k)
-    for k in range(nz):
-        each_block(0, k, early)
-        if k + 2 < nz:
-            take_on(0, k + 2)
-        if k == max(nz - 4, 0):
-            send_own(1)
-    take_on(1, 1)
-    order = list(range(nz - 1, -1, -1))
-    for k in order:
-        grad_send(k)
-    for k in range(2, nz):
-        take_on(1, k)
-    for k in order:
-        grad_own(k)
-    lax.fori_loop(0, nz, input_grad, 0)
-
-    tasks = []
-    for i in range(nz + 2):
-        chain = []
-        if i >= 2:
-            chain.append((grad_x_back, order[i - 2]))
-        if 1 <= i <= nz:
-            chain.append((grad_z, order[i - 1]))
-        if i < nz:
-            chain.append((grad_x, order[i]))
-        tasks.append(chain)
-    for i in range(nz + 2):
-        for task, k in tasks[i]:
-            task(k)
-        if i < nz:
-            each_block(1, i, late)
-        if i < nz - 1:
-            sum_pass(1, i)
-        if i == nz - 1:
-            sum_end(1)
-        if i >= 2 and i - 2 < nz - 1:
-            pass
-        if i == nz - 1:
-            for p in range(nz - 1):
-                sum_pass(0, p)
-        if i == nz:
-            sum_end(0)
-    for k in range(nz):
-        g_copy(k, 1 - r).wait_recv()
+            run("relay", relay, k - 1)
+    run("take_e", take_on, EARLY, 1)
+    run("relay", relay, last)
+    run("take_c", take_on, COT, 1)
+    for k in range(last):
+        run("gathered", gathered, k)
+    if last > 1:
+        run("take_e", take_on, EARLY, 2)
+    run("gathered", gathered, last)
+    run("early", early_level, 0)
+    if last > 1:
+        run("take_c", take_on, COT, 2)
+    for k in range(3, last):
+        run("take_e", take_on, EARLY, k)
+        run("take_c", take_on, COT, k)
+    run("send_l", send_own, LATE)
+    run("early", early_level, 1)
+    if last > 1:
+        run("input_grad", each_block, 0, input_grad)
+        run("input_grad", each_block, 1, input_grad)
+    for k in range(2, last):
+        run("early", early_level, k)
+        run("sum_e", sum_step, 1, k - 1, 0)
+        run("input_grad", each_block, k, input_grad)
+    if last > 2:
+        run("sum_e", sum_step, 1, last - 1, 0)
+        run("take_e", take_on, EARLY, last)
+        run("take_c", take_on, COT, last)
+    if last > 1:
+        run("early", early_level, last)
+    order = [(k, i) for k in range(last, -1, -1) for i in range(3)]
+    def send_next(count):
+        for _ in range(count):
+            if to_send:
+                run("grad_send", grad_send, *to_send.pop(0))
+
+    def own_next(count):
+        for _ in range(count):
+            if to_own:
+                run("grad_own", grad_own, *to_own.pop(0))
+
+    to_send, to_own = list(order), list(order)
+    send_next(4)
+    run("take_l", take_on, LATE, 1)
+    for copy in local_sums:
+        copy.wait()
+    if last == 1:
+        run("input_grad", each_block, 0, input_grad)
+    if last == 2:
+        run("sum_e", sum_step, 1, 1, 0)
+    run("input_grad", each_block, last, input_grad)
+    send_next(1)
+    own_next(2)
+    run("sum_e", sum_step, 1, last, 0)
+    send_next(1)
+    run("late", late_level, 0)
+    run("late", late_level, 1)
+
+    between = {}
+
+    def place(j, *task):
+        between.setdefault(j, []).append(task)
+
+    for far in range(2, nz):
+        place(3 * (far - 2), "take_l", take_on, LATE, far)
+        place(3 * (far - 2) + 1, "late", late_level, far)
+        for h in range(1, far):
+            place(2 * (far - 2) - 1 + 4 * (h - 1), "sum_e", sum_step, 1, far, h)
+            place(2 * (far - 2) + 7 + 3 * (h - 1), "sum_l", sum_step, 0, far, h)
+    for far in range(1, nz):
+        place(far + 2, "sum_l", sum_step, 0, far, 0)
+    place(6 * last - 10, "sum_end_e", sum_end, 1)
+    place(5 * last, "sum_end_l", sum_end, 0)
+    count, lag = len(order), 5
+    for j in range(min(min(between), -1), max(max(between), count + lag - 1) + 1):
+        if 0 <= j < count:
+            own_next(1)
+            run("grad_x", grad_x, *order[j])
+            send_next(1)
+        if 1 <= j <= count:
+            run("grad_z", grad_z, *order[j - 1])
+            if order[j - 1][0] == 0:
+                run("grad_back", grad_back, *order[j - 1])
+        if lag <= j < count + lag and order[j - lag][0]:
+            run("grad_back", grad_back, *order[j - lag])
+        for name, task, *args in between.get(j, ()):
+            run(name, task, *args)
+    for k, i in order:
+        run("grad_last", grad_last, k, i)
     for o in range(2):
         other = outs[o].at[half(1 - t), :]
         remote(other, other, os_.at[o], or_.at[o], to_t).wait_recv()
@@ -372,7 +464,7 @@
 
             @pl.when(z != b)
             def _():
-                sum_copy(o, 0, b).wait_send()
+                sum_copy(o, 0, b, to_t).wait_send()
 
     for condition, copy in pending:
         if condition is None:
@@ -383,7 +475,30 @@
                 copy.wait_send()
 
 
+def close_kernel(*refs):
+    sems = refs[-1]
+    count = (len(refs) - 1) // 2
+    copies = [pltpu.make_async_copy(refs[i], refs[count + i], sems.at[i]) for i in range(count)]
+    for copy in copies:
+        copy.start()
+    for copy in copies:
+        copy.wait()
+
+
+def close(*arrays):
+    return pl.pallas_call(
+        close_kernel,
+        out_shape=tuple(jax.ShapeDtypeStruct(a.shape, a.dtype) for a in arrays),
+        in_specs=[VMEM] * len(arrays),
+        out_specs=(HBM,) * len(arrays),
+        scratch_shapes=[dma(len(arrays))],
+        compiler_params=pltpu.CompilerParams(vmem_limit_bytes=8 * 2**20),
+        name="close",
+    )(*arrays)
+
+
 VMEM = pl.BlockSpec(memory_space=pltpu.VMEM)
+HBM = pl.BlockSpec(memory_space=pltpu.HBM)
 
 
 def dma(*shape):
@@ -407,24 +522,27 @@
     dl, ff = gate_weight.shape
     nz = n // 2
     u, q, hr = ff // nz, m // 2, dl // 2
-    later_output, earlier_input_grad, total = pl.pallas_call(
+    results = pl.pallas_call(
         functools.partial(fused_kernel, nz),
         out_shape=(
             jax.ShapeDtypeStruct((m, width), bf16),
             jax.ShapeDtypeStruct((m, width), bf16),
-            jax.ShapeDtypeStruct((3, dl, ff), bf16),
+            jax.ShapeDtypeStruct((dl, ff), f32),
+            jax.ShapeDtypeStruct((dl, ff), f32),
+            jax.ShapeDtypeStruct((dl, ff), f32),
         ),
-        in_specs=[VMEM] * 6,
-        out_specs=(VMEM, VMEM, VMEM),
+        in_specs=[HBM] * 9,
+        out_specs=(VMEM,) * 5,
         scratch_shapes=[
             pltpu.VMEM((3, nz, m, width), bf16),
+            pltpu.VMEM((3, dl, ff), bf16),
             pltpu.VMEM((3, width, u), bf16),
+            pltpu.VMEM((3, dl, ff), bf16),
             pltpu.VMEM((3, nz, m, u), bf16),
             pltpu.VMEM((2, nz, m, width), bf16),
             pltpu.VMEM((2, nz, q, width), bf16),
             pltpu.VMEM((2, 2, nz, q, width), bf16),
             pltpu.VMEM((2, nz, q, width), bf16),
-            pltpu.VMEM((q, width), f32),
             pltpu.VMEM((nz, 3, dl, u), f32),
             pltpu.VMEM((nz, 3, dl, u), bf16),
             pltpu.VMEM((nz, 3, dl, u), bf16),
@@ -432,18 +550,23 @@
             pltpu.VMEM((nz, 3, hr, u), bf16),
             pltpu.VMEM((nz, 3, hr, u), bf16),
         ]
+        + [dma(3)] * 4
         + [dma(nz)] * 2
         + [dma(nz, 2)] * 4
-        + [dma(2, 2), dma(2, nz, 2), dma(2, nz), dma(2, nz, 2), dma(2, nz, 2)]
+        + [dma(3, 2), dma(3, nz, 2), dma(3, nz), dma(3, nz, 2), dma(3, nz, 2)]
         + [dma(2, nz), dma(2, nz), dma(2, nz), dma(2, 2, nz), dma(2), dma(2)]
-        + [dma(nz)] * 8,
+        + [dma(nz, 3)] * 8,
         compiler_params=pltpu.CompilerParams(
-            collective_id=0, has_side_effects=True, vmem_limit_bytes=50 * 2**20
+            collective_id=0, has_side_effects=True, vmem_limit_bytes=44 * 2**20
         ),
         name="fused",
-    )(later_input, earlier_input, cotangent, gate_weight, up_weight, down_weight)
-    sums = tuple(old + total[i].astype(f32) for i, old in enumerate((gate_sum, up_sum, down_sum)))
-    return (later_output, earlier_input_grad) + sums
+    )(
+        *(
+            pltpu.with_memory_space_constraint(a, pltpu.HBM)
+            for a in (later_input, earlier_input, cotangent, gate_weight, up_weight, down_weight, gate_sum, up_sum, down_sum)
+        )
+    )
+    return close(*results)
 
 
 def early_parts(gate_early, up_early, hidden_grad):
@@ -549,7 +672,7 @@
             and layers & (layers - 1) == 0
             and units % (layers * 128) == 0
             and depth % 128 == 0
-            and rows % 32 == 0
+            and rows % 64 == 0
             and arrays[0].shape[1] % 512 == 0
             and arrays[0].shape[1] == depth * shards
         )

time: 176 us -> 143 us (0.81)
  Pallas kernels: 165 us -> 142 us
  local copies, waits for them, and re-layouts: 5.84 us -> 0 us
  other arithmetic: 4.5 us -> 0 us
    pallas_call x1, Pallas kernels: 165 us -> 139 us  [split_hidden(): pl.pallas_call(functools.partial(fused_kernel, nz), out_shape=(jax.ShapeD...]
    unnamed x14 -> x0, local copies, waits for them, and re-layouts: 5.84 us -> none
    add x1 -> x0, other arithmetic: 4.5 us -> none  [split_hidden(): old + total[i].astype(f32)]
    pallas_call x0 -> x1, Pallas kernels: none -> 2.57 us  [close(): pl.pallas_call(close_kernel, out_shape=tuple((jax.ShapeDtypeStruct(a.shap...]
where the time goes in v2:
time: 143 us; the launch traced here: 142 us
  Pallas kernels  142 us (99%)
    pallas_call x1, Pallas kernels, split_hidden(): pl.pallas_call(functools.partial(fused_kernel, nz), out_shape=(jax.ShapeD...  139 us

profile of v2, /device:TPU:0, one launch (start us, length us, event | category | flops | bytes accessed | tf_op | source)
XLA Modules:
  0.0 142.4 jit_solution(13251859638985390002)
XLA Ops:
  0.6 139.0 %fused.1 = (bf16[128,2048]{1,0:T(8,128)(2,1)S(1)}, bf16[128,2048]{1,0:T(8,128)(2,1)S(1)}, f32[256,1536]{1,0:T(8,128)S(1)}, f32[256,1536]{1,0:T(8,128)S(1)}, f32[256,1536]{1,0:T(8,128)S(1)}) custom-call(bf16[128,2048]{1,0:T(8,128)(2,1)} %later.1, bf16[128,2048]{1,0:T(8,128)(2,1)} %earlier.1, bf16[128,2048]{1,0:T(8,128)(2,1)} %cot.1, bf16[256,1536]{1,0:T(8,128)(2,1)} %gw.1, ...), custom_call_target="tpu_custom_call" | custom-call | tf_op jit(solution)/shard_map/fused/pallas_call | solution.py:525
  139.7 2.6 %close.1 = (bf16[128,2048]{1,0:T(8,128)(2,1)}, bf16[128,2048]{1,0:T(8,128)(2,1)}, f32[256,1536]{1,0:T(8,128)}, f32[256,1536]{1,0:T(8,128)}, f32[256,1536]{1,0:T(8,128)}) custom-call(bf16[128,2048]{1,0:T(8,128)(2,1)S(1)} %get-tuple-element.10.refs_0_, bf16[128,2048]{1,0:T(8,128)(2,1)S(1)} %get-tuple-element.11.refs_1_, ...), custom_call_target="tpu_custom_call" | custom-call | tf_op jit(solution)/shard_map/close/pallas_call | solution.py:489

commit v3 on v2

--- a/solution.py
+++ b/solution.py
@@ -39,7 +39,7 @@
 
 def fused_kernel(
     nz, later, earlier, cot, gw, uw, dw, gsum, usum, dsum, late_out, early_out, gnew, unew, dnew,
-    slots, wt, w, g_out, hid, part, peer, rin, rout, gown, gyo, gyi, gxo, gxi, gzo,
+    slots, wt, w, g_out, hid, part, peer, rin, rout, gown, gboth, gyo, gyi, gxo, gxi, gzo,
     lts, lws, los, lns, wzs, wzr, wxs, wxr, wys, wyr, aos, ags, agr, cs, cr,
     tds, tdr, rss, rsr, os_, or_, gys, gyr, gxs, gxr, gzs, gzr, gfs, gfr,
 ):
@@ -48,7 +48,7 @@
     m, width = later.shape
     q = m // 2
     dl, u = gw.shape[0], w.shape[2]
-    hr = dl // 2
+    hr, last = dl // 2, nz - 1
     f32, bf16 = jnp.float32, jnp.bfloat16
     outs = (late_out, early_out)
     to_x, to_y, to_t = {"rep": 1 - r}, {"fs": z * 2 + 1 - y}, {"tp": 1 - t}
@@ -99,30 +99,30 @@
         return w.at[:, rows(side, height, h), :]
 
     def send_weights(height, send, recv, device):
-        go(remote(wt.at[:, span(r * hr, hr, hr), units(height)], piece(y, z, r), send, recv, device))
+        remote(wt.at[:, span(r * hr, hr, hr), units(height)], piece(y, z, r), send, recv, device).start()
 
     def wx(k, a, block):
-        return remote(block, block, wxs.at[k, a], wxr.at[k, a], to_x)
+        return remote(block, block, wxs.at[0], wxr.at[k, a], to_x)
 
     def wy(k, a, block):
-        return remote(block, block, wys.at[k, a], wyr.at[k, a], to_y)
+        return remote(block, block, wys.at[0], wyr.at[k, a], to_y)
 
     def spread(k):
         block = piece(y, flip(z, k, nz), r)
-        remote(block, block, wzs.at[k], wzr.at[k], to_x).wait_recv()
-        go(wx(k, 0, block))
-        go(wy(k, 0, block))
+        remote(block, block, wzs.at[0], wzr.at[k], to_x).wait_recv()
+        wx(k, 0, block).start()
+        wy(k, 0, block).start()
 
     def relay(k):
         height = flip(z, k, nz)
         if k % 2:
             block = piece(y, height, 1 - r)
             wx(k, 0, block).wait_recv()
-            go(wy(k, 1, block))
+            wy(k, 1, block).start()
         else:
             block = piece(1 - y, height, r)
             wy(k, 0, block).wait_recv()
-            go(wx(k, 1, block))
+            wx(k, 1, block).start()
 
     def gathered(k):
         height = flip(z, k, nz)
@@ -146,33 +146,41 @@
     def exists(height):
         return jnp.logical_and(height >= 0, height < nz)
 
-    def send_own(g):
+    def send_own(g, ends=None):
         for d in range(2):
             target = z + step_of(d)
             block = block_of(g, z, t)
-            when_go(exists(target), remote(block, block, aos.at[g, d], agr.at[g, z], layer(target)))
+            at_end = z == (last if d else 0)
+            chosen = exists(target)
+            if ends is not None:
+                chosen = jnp.logical_and(chosen, at_end if ends else jnp.logical_not(at_end))
+            when_go(chosen, remote(block, block, aos.at[g, d], agr.at[g, z], layer(target)))
 
     def take_on(g, k):
         for d in range(2):
             origin, target = z - step_of(d) * k, z + step_of(d)
             block = block_of(g, origin, t)
-            ahead = remote(block, block, ags.at[g, k, d], agr.at[g, origin], layer(target))
-            over = remote(block, block, cs.at[g, k, d], cr.at[g, k, d], to_t)
+            ahead = remote(block, block, ags.at[g, min(k, last - 1), d], agr.at[g, origin], layer(target))
 
             @pl.when(exists(origin))
             def _():
                 ahead.wait_recv()
 
-            when_go(jnp.logical_and(exists(origin), exists(target)), ahead)
-            when_go(exists(origin), over)
+            if k < last:
+                when_go(jnp.logical_and(exists(origin), exists(target)), ahead)
+
+            @pl.when(exists(origin))
+            def _():
+                remote(block, block, cs.at[0], cr.at[g, origin], to_t).start()
 
     def whole(g, k):
         for d in range(2):
-            block = block_of(g, z - step_of(d) * k, 1 - t)
-
-            @pl.when(exists(z - step_of(d) * k))
+            origin = z - step_of(d) * k
+            block = block_of(g, origin, 1 - t)
+
+            @pl.when(exists(origin))
             def _():
-                remote(block, block, cs.at[g, k, d], cr.at[g, k, d], to_t).wait_recv()
+                remote(block, block, cs.at[0], cr.at[g, origin], to_t).wait_recv()
 
     def each_block(k, body):
         if k == 0:
@@ -205,7 +213,7 @@
     step = width // 4
 
     def trade(o, b):
-        return remote(part.at[o, b, half(1 - t), :], peer.at[o, b], tds.at[o, b], tdr.at[o, b], to_t)
+        return remote(part.at[o, b, half(1 - t), :], peer.at[o, b], tds.at[0], tdr.at[o, b], to_t)
 
     def late(b):
         gate = jnp.dot(slots[0, b], w[0], preferred_element_type=f32)
@@ -232,7 +240,7 @@
     fine = 16
 
     def traded(o, b):
-        remote(peer.at[o, b], peer.at[o, b], tds.at[o, b], tdr.at[o, b], to_t).wait_recv()
+        remote(peer.at[o, b], peer.at[o, b], tds.at[0], tdr.at[o, b], to_t).wait_recv()
 
     def chunks(body):
         def one(i, carry):
@@ -248,7 +256,7 @@
         )
 
     def sum_copy(o, d, b, device):
-        return remote(rout.at[o, b], rin.at[d, o, b], rss.at[o, b], rsr.at[d, o, b], device)
+        return remote(rout.at[o, b], rin.at[d, o, b], rss.at[0], rsr.at[d, o, b], device)
 
     def sum_step(o, far, h):
         @pl.when(jnp.logical_or(z == h, z == nz - 1 - h))
@@ -298,7 +306,7 @@
 
     def grad_send(k, i):
         gyo[k, i] = grad_block(1 - y, flip(z, k, nz), i).astype(bf16)
-        go(remote(gyo.at[k, i], gyi.at[k, i], gys.at[k, i], gyr.at[k, i], to_y))
+        remote(gyo.at[k, i], gyi.at[k, i], gys.at[0], gyr.at[k, i], to_y).start()
 
     def grad_own(k, i):
         gown[k, i] = grad_block(y, flip(z, k, nz), i)
@@ -306,33 +314,54 @@
     mine_rows, their_rows = span(r * hr, hr, hr), span((1 - r) * hr, hr, hr)
 
     def grad_x(k, i):
-        remote(gyi.at[k, i], gyi.at[k, i], gys.at[k, i], gyr.at[k, i], to_y).wait_recv()
+        remote(gyi.at[k, i], gyi.at[k, i], gys.at[0], gyr.at[k, i], to_y).wait_recv()
         gxo[k, i] = (gown[k, i, their_rows, :] + gyi[k, i, their_rows, :].astype(f32)).astype(bf16)
-        go(remote(gxo.at[k, i], gxi.at[k, i], gxs.at[k, i], gxr.at[k, i], to_x))
+        remote(gxo.at[k, i], gxi.at[k, i], gxs.at[0], gxr.at[k, i], to_x).start()
+
+    def cross_x(i):
+        return remote(gyo.at[0, i], gyi.at[0, i], gys.at[0], gyr.at[0, i], to_x)
+
+    def cross_y(i):
+        return remote(gxo.at[0, i], gxi.at[0, i], gxs.at[0], gxr.at[0, i], to_y)
+
+    def cross_send(i):
+        for s, side in enumerate((y, 1 - y)):
+            gboth[s, i] = grad_block(side, z, i)
+            gyo[0, i, s * hr:(s + 1) * hr, :] = gboth[s, i, their_rows, :].astype(bf16)
+        cross_x(i).start()
+
+    def cross_turn(i):
+        cross_x(i).wait_recv()
+        gxo[0, i] = (gboth[1, i, mine_rows, :] + gyi[0, i, hr:, :].astype(f32)).astype(bf16)
+        cross_y(i).start()
+
+    def cross_end(i):
+        cross_y(i).wait_recv()
+        g_out[i, mine_rows, units(z)] = (
+            gboth[0, i, mine_rows, :] + gyi[0, i, :hr, :].astype(f32) + gxi[0, i].astype(f32)
+        ).astype(bf16)
+        grad_back(0, i)
 
     def g_block(i, height, h):
         return g_out.at[i, span(h * hr, hr, hr), units(height)]
 
     def grad_z(k, i):
-        remote(gxi.at[k, i], gxi.at[k, i], gxs.at[k, i], gxr.at[k, i], to_x).wait_recv()
+        remote(gxi.at[k, i], gxi.at[k, i], gxs.at[0], gxr.at[k, i], to_x).wait_recv()
         total = (
             gown[k, i, mine_rows, :] + gyi[k, i, mine_rows, :].astype(f32) + gxi[k, i].astype(f32)
         ).astype(bf16)
-        if k:
-            gzo[k, i] = total
-            go(remote(gzo.at[k, i], g_block(i, z, r), gzs.at[k, i], gzr.at[k, i], layer(flip(z, k, nz))))
-        else:
-            g_out[i, mine_rows, units(z)] = total
+        gzo[k, i] = total
+        remote(gzo.at[k, i], g_block(i, z, r), gzs.at[0], gzr.at[k, i], layer(flip(z, k, nz))).start()
 
     def g_copy(k, i, h):
         block = g_block(i, flip(z, k, nz), h)
-        return remote(block, block, gfs.at[k, i], gfr.at[k, i], to_x)
+        return remote(block, block, gfs.at[0], gfr.at[k, i], to_x)
 
     def grad_back(k, i):
         if k:
             block = g_block(i, flip(z, k, nz), r)
-            remote(block, block, gzs.at[k, i], gzr.at[k, i], to_x).wait_recv()
-        go(g_copy(k, i, r))
+            remote(block, block, gzs.at[0], gzr.at[k, i], to_x).wait_recv()
+        g_copy(k, i, r).start()
         grad_add(k, i, r)
 
     def grad_add(k, i, h):
@@ -351,16 +380,16 @@
         for copy in local_weights:
             copy.wait()
         for k in range(1, nz):
-            send_weights(flip(z, k, nz), wzs.at[k], wzr.at[k], layer(flip(z, k, nz)))
-        send_weights(z, wys.at[0, 0], wyr.at[0, 0], to_y)
+            send_weights(flip(z, k, nz), wzs.at[0], wzr.at[k], layer(flip(z, k, nz)))
+        send_weights(z, wys.at[0], wyr.at[0, 0], to_y)
         for copy in local_tokens:
             copy.wait()
         send_own(EARLY)
         send_own(COT)
+        send_own(LATE, True)
         for copy in local_own:
             copy.wait()
 
-    last = nz - 1
     run("send_first", send_first)
     run("relay", relay, 0)
     for k in range(1, nz):
@@ -381,7 +410,7 @@
     for k in range(3, last):
         run("take_e", take_on, EARLY, k)
         run("take_c", take_on, COT, k)
-    run("send_l", send_own, LATE)
+    run("send_l", send_own, LATE, False)
     run("early", early_level, 1)
     if last > 1:
         run("input_grad", each_block, 0, input_grad)
@@ -396,7 +425,7 @@
         run("take_c", take_on, COT, last)
     if last > 1:
         run("early", early_level, last)
-    order = [(k, i) for k in range(last, -1, -1) for i in range(3)]
+    order = [(k, i) for k in range(last, 0, -1) for i in range(3)]
     def send_next(count):
         for _ in range(count):
             if to_send:
@@ -408,19 +437,24 @@
                 run("grad_own", grad_own, *to_own.pop(0))
 
     to_send, to_own = list(order), list(order)
-    send_next(4)
+    send_next(1)
+    run("cross_send", cross_send, 0)
+    send_next(1)
+    run("cross_send", cross_send, 1)
+    if last == 1:
+        run("input_grad", each_block, 0, input_grad)
+    run("input_grad", each_block, last, input_grad)
+    send_next(1)
+    run("cross_send", cross_send, 2)
+    send_next(1)
+    if last == 2:
+        run("sum_e", sum_step, 1, 1, 0)
+    run("sum_e", sum_step, 1, last, 0)
     run("take_l", take_on, LATE, 1)
+    send_next(1)
+    own_next(2)
     for copy in local_sums:
         copy.wait()
-    if last == 1:
-        run("input_grad", each_block, 0, input_grad)
-    if last == 2:
-        run("sum_e", sum_step, 1, 1, 0)
-    run("input_grad", each_block, last, input_grad)
-    send_next(1)
-    own_next(2)
-    run("sum_e", sum_step, 1, last, 0)
-    send_next(1)
     run("late", late_level, 0)
     run("late", late_level, 1)
 
@@ -429,50 +463,64 @@
     def place(j, *task):
         between.setdefault(j, []).append(task)
 
+    count, late_sums = len(order), []
+    for i in range(3):
+        place(i, "cross_turn", cross_turn, i)
+        place(i + 6, "cross_end", cross_end, i)
     for far in range(2, nz):
-        place(3 * (far - 2), "take_l", take_on, LATE, far)
-        place(3 * (far - 2) + 1, "late", late_level, far)
+        place(far - 2, "take_l", take_on, LATE, far)
+        place(far - 1, "late", late_level, far)
+        place(far, "sum_l", sum_step, 0, far, 0)
         for h in range(1, far):
-            place(2 * (far - 2) - 1 + 4 * (h - 1), "sum_e", sum_step, 1, far, h)
-            place(2 * (far - 2) + 7 + 3 * (h - 1), "sum_l", sum_step, 0, far, h)
-    for far in range(1, nz):
-        place(far + 2, "sum_l", sum_step, 0, far, 0)
-    place(6 * last - 10, "sum_end_e", sum_end, 1)
-    place(5 * last, "sum_end_l", sum_end, 0)
-    count, lag = len(order), 5
-    for j in range(min(min(between), -1), max(max(between), count + lag - 1) + 1):
+            place(2 * (far - 2) - 1 + 5 * (h - 1), "sum_e", sum_step, 1, far, h)
+            late_sums.append((far + 3 + (6 if h > 1 else 1) * (h - 1), far, h))
+    place(0, "sum_l", sum_step, 0, 1, 0)
+    place(2 * last + 2, "sum_end_e", sum_end, 1)
+    for j, (k, i) in enumerate(order):
+        place(j + (5 if k == last else 6 if k > 1 else 4), "grad_back", grad_back, k, i)
+    for j, far, h in late_sums:
+        place(j, "sum_l", sum_step, 0, far, h)
+    place(count + 3, "sum_end_l", sum_end, 0)
+    for j in range(min(min(between), -1), max(max(between), count) + 1):
         if 0 <= j < count:
             own_next(1)
             run("grad_x", grad_x, *order[j])
             send_next(1)
         if 1 <= j <= count:
             run("grad_z", grad_z, *order[j - 1])
-            if order[j - 1][0] == 0:
-                run("grad_back", grad_back, *order[j - 1])
-        if lag <= j < count + lag and order[j - lag][0]:
-            run("grad_back", grad_back, *order[j - lag])
         for name, task, *args in between.get(j, ()):
             run(name, task, *args)
-    for k, i in order:
+    for k, i in [(0, 0), (0, 1), (0, 2)] + order:
         run("grad_last", grad_last, k, i)
-    for o in range(2):
-        other = outs[o].at[half(1 - t), :]
-        remote(other, other, os_.at[o], or_.at[o], to_t).wait_recv()
-    for o in range(2):
-        for b in range(nz):
-            trade(o, b).wait_send()
-
-            @pl.when(z != b)
-            def _():
-                sum_copy(o, 0, b, to_t).wait_send()
-
-    for condition, copy in pending:
-        if condition is None:
-            copy.wait_send()
-        else:
-            @pl.when(condition)
-            def _():
+    def finish():
+        for o in range(2):
+            other = outs[o].at[half(1 - t), :]
+            remote(other, other, os_.at[o], or_.at[o], to_t).wait_recv()
+
+    def drain():
+        def sent(block, sem):
+            remote(block, block, sem.at[0], sem.at[0], to_t).wait_send()
+
+        sent(w.at[:, pl.ds(0, last * hr), :], wzs)
+        sent(w.at[:, pl.ds(0, (last + nz // 2) * hr), :], wxs)
+        sent(w.at[:, pl.ds(0, (nz + nz // 2) * hr), :], wys)
+        sent(slots.at[:, pl.ds(0, last), pl.ds(0, q), :], cs)
+        sent(peer, tds)
+        sent(rout.at[:, pl.ds(0, last)], rss)
+        sent(gyo, gys)
+        sent(gxo, gxs)
+        sent(gzo.at[pl.ds(1, last)], gzs)
+        sent(gxo, gfs)
+        for condition, copy in pending:
+            if condition is None:
                 copy.wait_send()
+            else:
+                @pl.when(condition)
+                def _():
+                    copy.wait_send()
+
+    run("finish", finish)
+    run("drain", drain)
 
 
 def close_kernel(*refs):
@@ -544,6 +592,7 @@
             pltpu.VMEM((2, 2, nz, q, width), bf16),
             pltpu.VMEM((2, nz, q, width), bf16),
             pltpu.VMEM((nz, 3, dl, u), f32),
+            pltpu.VMEM((2, 3, dl, u), f32),
             pltpu.VMEM((nz, 3, dl, u), bf16),
             pltpu.VMEM((nz, 3, dl, u), bf16),
             pltpu.VMEM((nz, 3, hr, u), bf16),
@@ -551,13 +600,12 @@
             pltpu.VMEM((nz, 3, hr, u), bf16),
         ]
         + [dma(3)] * 4
-        + [dma(nz)] * 2
-        + [dma(nz, 2)] * 4
-        + [dma(3, 2), dma(3, nz, 2), dma(3, nz), dma(3, nz, 2), dma(3, nz, 2)]
-        + [dma(2, nz), dma(2, nz), dma(2, nz), dma(2, 2, nz), dma(2), dma(2)]
-        + [dma(nz, 3)] * 8,
+        + [dma(1), dma(nz), dma(1), dma(nz, 2), dma(1), dma(nz, 2)]
+        + [dma(3, 2), dma(3, max(nz - 1, 1), 2), dma(3, nz), dma(1), dma(3, nz)]
+        + [dma(1), dma(2, nz), dma(1), dma(2, 2, nz), dma(2), dma(2)]
+        + [dma(1), dma(nz, 3)] * 4,
         compiler_params=pltpu.CompilerParams(
-            collective_id=0, has_side_effects=True, vmem_limit_bytes=44 * 2**20
+            collective_id=0, has_side_effects=True, vmem_limit_bytes=46 * 2**20
         ),
         name="fused",
     )(

time: 143 us -> 136 us (0.951)
  Pallas kernels: 142 us -> 135 us
    pallas_call x1, Pallas kernels: 139 us -> 132 us  [split_hidden(): pl.pallas_call(functools.partial(fused_kernel, nz), out_shape=(jax.ShapeD...]
where the time goes in v3:
time: 136 us
  Pallas kernels  135 us (99%)
    pallas_call x1, Pallas kernels, split_hidden(): pl.pallas_call(functools.partial(fused_kernel, nz), out_shape=(jax.ShapeD...  132 us

profile of v3, /device:TPU:0, one launch (start us, length us, event | category | flops | bytes accessed | tf_op | source)
XLA Modules:
  0.0 135.6 jit_solution(11365513181317091376)
XLA Ops:
  0.6 132.2 %fused.1 = (bf16[128,2048]{1,0:T(8,128)(2,1)S(1)}, bf16[128,2048]{1,0:T(8,128)(2,1)S(1)}, f32[256,1536]{1,0:T(8,128)S(1)}, f32[256,1536]{1,0:T(8,128)S(1)}, f32[256,1536]{1,0:T(8,128)S(1)}) custom-call(bf16[128,2048]{1,0:T(8,128)(2,1)} %later.1, bf16[128,2048]{1,0:T(8,128)(2,1)} %earlier.1, bf16[128,2048]{1,0:T(8,128)(2,1)} %cot.1, bf16[256,1536]{1,0:T(8,128)(2,1)} %gw.1, ...), custom_call_target="tpu_custom_call" | custom-call | tf_op jit(solution)/shard_map/fused/pallas_call | solution.py:573
  132.9 2.6 %close.1 = (bf16[128,2048]{1,0:T(8,128)(2,1)}, bf16[128,2048]{1,0:T(8,128)(2,1)}, f32[256,1536]{1,0:T(8,128)}, f32[256,1536]{1,0:T(8,128)}, f32[256,1536]{1,0:T(8,128)}) custom-call(bf16[128,2048]{1,0:T(8,128)(2,1)S(1)} %get-tuple-element.10.refs_0_, bf16[128,2048]{1,0:T(8,128)(2,1)S(1)} %get-tuple-element.11.refs_1_, ...), custom_call_target="tpu_custom_call" | custom-call | tf_op jit(solution)/shard_map/close/pallas_call | solution.py:537

commit v4 on v3

--- a/solution.py
+++ b/solution.py
@@ -39,7 +39,7 @@
 
 def fused_kernel(
     nz, later, earlier, cot, gw, uw, dw, gsum, usum, dsum, late_out, early_out, gnew, unew, dnew,
-    slots, wt, w, g_out, hid, part, peer, rin, rout, gown, gboth, gyo, gyi, gxo, gxi, gzo,
+    slots, wt, w, g_out, hid, part, peer, rin, rout, gown, gside, gother, gyo, gyi, gxo, gxi, gzo,
     lts, lws, los, lns, wzs, wzr, wxs, wxr, wys, wyr, aos, ags, agr, cs, cr,
     tds, tdr, rss, rsr, os_, or_, gys, gyr, gxs, gxr, gzs, gzr, gfs, gfr,
 ):
@@ -156,20 +156,24 @@
                 chosen = jnp.logical_and(chosen, at_end if ends else jnp.logical_not(at_end))
             when_go(chosen, remote(block, block, aos.at[g, d], agr.at[g, z], layer(target)))
 
-    def take_on(g, k):
+    def take_on(g, k, ends=None):
         for d in range(2):
             origin, target = z - step_of(d) * k, z + step_of(d)
             block = block_of(g, origin, t)
             ahead = remote(block, block, ags.at[g, min(k, last - 1), d], agr.at[g, origin], layer(target))
-
-            @pl.when(exists(origin))
+            chosen = exists(origin)
+            if ends is not None:
+                at_end = origin == (last if d else 0)
+                chosen = jnp.logical_and(chosen, at_end if ends else jnp.logical_not(at_end))
+
+            @pl.when(chosen)
             def _():
                 ahead.wait_recv()
 
             if k < last:
-                when_go(jnp.logical_and(exists(origin), exists(target)), ahead)
-
-            @pl.when(exists(origin))
+                when_go(jnp.logical_and(chosen, exists(target)), ahead)
+
+            @pl.when(chosen)
             def _():
                 remote(block, block, cs.at[0], cr.at[g, origin], to_t).start()
 
@@ -318,29 +322,37 @@
         gxo[k, i] = (gown[k, i, their_rows, :] + gyi[k, i, their_rows, :].astype(f32)).astype(bf16)
         remote(gxo.at[k, i], gxi.at[k, i], gxs.at[0], gxr.at[k, i], to_x).start()
 
-    def cross_x(i):
-        return remote(gyo.at[0, i], gyi.at[0, i], gys.at[0], gyr.at[0, i], to_x)
-
-    def cross_y(i):
-        return remote(gxo.at[0, i], gxi.at[0, i], gxs.at[0], gxr.at[0, i], to_y)
-
-    def cross_send(i):
-        for s, side in enumerate((y, 1 - y)):
-            gboth[s, i] = grad_block(side, z, i)
-            gyo[0, i, s * hr:(s + 1) * hr, :] = gboth[s, i, their_rows, :].astype(bf16)
-        cross_x(i).start()
-
-    def cross_turn(i):
-        cross_x(i).wait_recv()
-        gxo[0, i] = (gboth[1, i, mine_rows, :] + gyi[0, i, hr:, :].astype(f32)).astype(bf16)
-        cross_y(i).start()
-
-    def cross_end(i):
-        cross_y(i).wait_recv()
-        g_out[i, mine_rows, units(z)] = (
-            gboth[0, i, mine_rows, :] + gyi[0, i, :hr, :].astype(f32) + gxi[0, i].astype(f32)
-        ).astype(bf16)
-        grad_back(0, i)
+    def cross_x(k, i):
+        return remote(gyo.at[k, i], gyi.at[k, i], gys.at[0], gyr.at[k, i], to_x)
+
+    def cross_y(k, i):
+        return remote(gxo.at[k, i], gxi.at[k, i], gxs.at[0], gxr.at[k, i], to_y)
+
+    def cross_send(k, i, c):
+        gown[k, i] = grad_block(y, flip(z, k, nz), i)
+        gyo[k, i, :hr, :] = gown[k, i, their_rows, :].astype(bf16)
+        gside[...] = grad_block(1 - y, flip(z, k, nz), i)
+        gyo[k, i, hr:, :] = gside[their_rows, :].astype(bf16)
+        gother[c] = gside[mine_rows, :]
+        cross_x(k, i).start()
+
+    def cross_turn(k, i, c):
+        cross_x(k, i).wait_recv()
+        gxo[k, i] = (gother[c] + gyi[k, i, hr:, :].astype(f32)).astype(bf16)
+        cross_y(k, i).start()
+
+    def cross_end(k, i, c):
+        cross_y(k, i).wait_recv()
+        total = (gown[k, i, mine_rows, :] + gyi[k, i, :hr, :].astype(f32) + gxi[k, i].astype(f32)).astype(bf16)
+        if k:
+            gzo[k, i] = total
+            grad_onward(k, i)
+        else:
+            g_out[i, mine_rows, units(z)] = total
+            grad_back(k, i)
+
+    def grad_onward(k, i):
+        remote(gzo.at[k, i], g_block(i, z, r), gzs.at[0], gzr.at[k, i], layer(flip(z, k, nz))).start()
 
     def g_block(i, height, h):
         return g_out.at[i, span(h * hr, hr, hr), units(height)]
@@ -351,7 +363,7 @@
             gown[k, i, mine_rows, :] + gyi[k, i, mine_rows, :].astype(f32) + gxi[k, i].astype(f32)
         ).astype(bf16)
         gzo[k, i] = total
-        remote(gzo.at[k, i], g_block(i, z, r), gzs.at[0], gzr.at[k, i], layer(flip(z, k, nz))).start()
+        grad_onward(k, i)
 
     def g_copy(k, i, h):
         block = g_block(i, flip(z, k, nz), h)
@@ -411,26 +423,30 @@
         run("take_e", take_on, EARLY, k)
         run("take_c", take_on, COT, k)
     run("send_l", send_own, LATE, False)
-    run("early", early_level, 1)
-    if last > 1:
-        run("input_grad", each_block, 0, input_grad)
-        run("input_grad", each_block, 1, input_grad)
-    for k in range(2, last):
+    run("take_l_end", take_on, LATE, 1, True)
+    for k in range(last - 1, 0, -1):
         run("early", early_level, k)
-        run("sum_e", sum_step, 1, k - 1, 0)
+        if 1 < k + 1 < last:
+            run("sum_e", sum_step, 1, k + 1, 0)
         run("input_grad", each_block, k, input_grad)
     if last > 2:
-        run("sum_e", sum_step, 1, last - 1, 0)
         run("take_e", take_on, EARLY, last)
         run("take_c", take_on, COT, last)
+    if last == 1:
+        run("early", early_level, 1)
     if last > 1:
         run("early", early_level, last)
-    order = [(k, i) for k in range(last, 0, -1) for i in range(3)]
+    crossing = [(0, 0), (0, 1), (0, 2)] + [(1, i) for i in range(1)]
+    order = [(k, i) for k in range(last, 0, -1) for i in range(3) if (k, i) not in crossing]
     def send_next(count):
         for _ in range(count):
             if to_send:
                 run("grad_send", grad_send, *to_send.pop(0))
 
+    def wait_sums():
+        for copy in local_sums:
+            copy.wait()
+
     def own_next(count):
         for _ in range(count):
             if to_own:
@@ -438,49 +454,52 @@
 
     to_send, to_own = list(order), list(order)
     send_next(1)
-    run("cross_send", cross_send, 0)
+    run("cross_send", cross_send, *crossing[0], 0)
     send_next(1)
-    run("cross_send", cross_send, 1)
-    if last == 1:
-        run("input_grad", each_block, 0, input_grad)
+    run("cross_send", cross_send, *crossing[1], 1)
     run("input_grad", each_block, last, input_grad)
-    send_next(1)
-    run("cross_send", cross_send, 2)
-    send_next(1)
-    if last == 2:
+    send_next(2)
+    run("take_l", take_on, LATE, 1, False)
+    run("sum_e", sum_step, 1, last, 0)
+    if last > 1:
         run("sum_e", sum_step, 1, 1, 0)
-    run("sum_e", sum_step, 1, last, 0)
-    run("take_l", take_on, LATE, 1)
+    run("input_grad", each_block, 0, input_grad)
     send_next(1)
     own_next(2)
-    for copy in local_sums:
-        copy.wait()
-    run("late", late_level, 0)
-    run("late", late_level, 1)
 
     between = {}
 
     def place(j, *task):
         between.setdefault(j, []).append(task)
 
-    count, late_sums = len(order), []
-    for i in range(3):
-        place(i, "cross_turn", cross_turn, i)
-        place(i + 6, "cross_end", cross_end, i)
+    count = len(order)
     for far in range(2, nz):
+        for h in range(1, far):
+            place(2 * far - 5 + 5 * (h - 1), "sum_e", sum_step, 1, far, h)
+    place(-1, "late", late_level, 1)
+    if last > 1:
+        place(-1, "take_l", take_on, LATE, 2)
+    place(-1, "late", late_level, 0)
+    for far in range(3, nz):
         place(far - 2, "take_l", take_on, LATE, far)
-        place(far - 1, "late", late_level, far)
-        place(far, "sum_l", sum_step, 0, far, 0)
+    for far in range(last, 0, -1):
+        if far > 1:
+            place(2 * (last - far) + 1, "late", late_level, far)
+        place(last - far + 2, "sum_l", sum_step, 0, far, 0)
         for h in range(1, far):
-            place(2 * (far - 2) - 1 + 5 * (h - 1), "sum_e", sum_step, 1, far, h)
-            late_sums.append((far + 3 + (6 if h > 1 else 1) * (h - 1), far, h))
-    place(0, "sum_l", sum_step, 0, 1, 0)
+            place(5 + 2 * (last - far) + 5 * (h - 1), "sum_l", sum_step, 0, far, h)
+    for c, (k, i) in enumerate(crossing):
+        if c > 1:
+            place(c, "cross_send", cross_send, k, i, c)
+        place((0, 2, 5, 6, 7, 8)[c], "cross_turn", cross_turn, k, i, c)
+        place((6, 7, 8, 8, 9, 9)[c], "cross_end", cross_end, k, i, c)
+        if k:
+            place((6, 7, 8, 8, 9, 9)[c] + 3, "grad_back", grad_back, k, i)
     place(2 * last + 2, "sum_end_e", sum_end, 1)
     for j, (k, i) in enumerate(order):
-        place(j + (5 if k == last else 6 if k > 1 else 4), "grad_back", grad_back, k, i)
-    for j, far, h in late_sums:
-        place(j, "sum_l", sum_step, 0, far, h)
-    place(count + 3, "sum_end_l", sum_end, 0)
+        place(j + (5 if k > 1 else 4), "grad_back", grad_back, k, i)
+    place(12, "sum_end_l", sum_end, 0)
+    place(-1, "sums", wait_sums)
     for j in range(min(min(between), -1), max(max(between), count) + 1):
         if 0 <= j < count:
             own_next(1)
@@ -490,7 +509,7 @@
             run("grad_z", grad_z, *order[j - 1])
         for name, task, *args in between.get(j, ()):
             run(name, task, *args)
-    for k, i in [(0, 0), (0, 1), (0, 2)] + order:
+    for k, i in crossing[:3] + order + crossing[3:]:
         run("grad_last", grad_last, k, i)
     def finish():
         for o in range(2):
@@ -592,7 +611,8 @@
             pltpu.VMEM((2, 2, nz, q, width), bf16),
             pltpu.VMEM((2, nz, q, width), bf16),
             pltpu.VMEM((nz, 3, dl, u), f32),
-            pltpu.VMEM((2, 3, dl, u), f32),
+            pltpu.VMEM((dl, u), f32),
+            pltpu.VMEM((6, hr, u), f32),
             pltpu.VMEM((nz, 3, dl, u), bf16),
             pltpu.VMEM((nz, 3, dl, u), bf16),
             pltpu.VMEM((nz, 3, hr, u), bf16),

time: 136 us -> 136 us (level)
  no operation moved by 1% of the time
where the time goes in v4:
time: 136 us; the launch traced here: 135 us
  Pallas kernels  135 us (99%)
    pallas_call x1, Pallas kernels, split_hidden(): pl.pallas_call(functools.partial(fused_kernel, nz), out_shape=(jax.ShapeD...  132 us

profile of v4, /device:TPU:0, one launch (start us, length us, event | category | flops | bytes accessed | tf_op | source)
XLA Modules:
  0.0 135.5 jit_solution(10136692935114892714)
XLA Ops:
  0.6 132.1 %fused.1 = (bf16[128,2048]{1,0:T(8,128)(2,1)S(1)}, bf16[128,2048]{1,0:T(8,128)(2,1)S(1)}, f32[256,1536]{1,0:T(8,128)S(1)}, f32[256,1536]{1,0:T(8,128)S(1)}, f32[256,1536]{1,0:T(8,128)S(1)}) custom-call(bf16[128,2048]{1,0:T(8,128)(2,1)} %later.1, bf16[128,2048]{1,0:T(8,128)(2,1)} %earlier.1, bf16[128,2048]{1,0:T(8,128)(2,1)} %cot.1, bf16[256,1536]{1,0:T(8,128)(2,1)} %gw.1, ...), custom_call_target="tpu_custom_call" | custom-call | tf_op jit(solution)/shard_map/fused/pallas_call | solution.py:592
  132.7 2.6 %close.1 = (bf16[128,2048]{1,0:T(8,128)(2,1)}, bf16[128,2048]{1,0:T(8,128)(2,1)}, f32[256,1536]{1,0:T(8,128)}, f32[256,1536]{1,0:T(8,128)}, f32[256,1536]{1,0:T(8,128)}) custom-call(bf16[128,2048]{1,0:T(8,128)(2,1)S(1)} %get-tuple-element.10.refs_0_, bf16[128,2048]{1,0:T(8,128)(2,1)S(1)} %get-tuple-element.11.refs_1_, ...), custom_call_target="tpu_custom_call" | custom-call | tf_op jit(solution)/shard_map/close/pallas_call | solution.py:556

commit v5 on v4

--- a/solution.py
+++ b/solution.py
@@ -64,14 +64,17 @@
         pltpu.make_async_copy(source, slots.at[slot_of[g], z], lts.at[g])
         for g, source in enumerate((earlier, cot, later))
     ]
-    local_weights = [pltpu.make_async_copy(source, wt.at[i], lws.at[i]) for i, source in enumerate((gw, uw, dw))]
+    local_weights = [
+        pltpu.make_async_copy(source.at[span(r * hr, hr, hr), :], wt.at[i], lws.at[i])
+        for i, source in enumerate((gw, uw, dw))
+    ]
     local_own = [
         pltpu.make_async_copy(source.at[:, units(z)], w.at[i, span((z * 2 + y) * dl, dl, dl), :], los.at[i])
         for i, source in enumerate((gw, uw, dw))
     ]
     news = (gnew, unew, dnew)
     local_sums = [pltpu.make_async_copy(source, news[i], lns.at[i]) for i, source in enumerate((gsum, usum, dsum))]
-    for copy in local_weights + local_tokens + local_own + local_sums:
+    for copy in local_weights:
         copy.start()
 
     barrier = pltpu.get_barrier_semaphore()
@@ -99,7 +102,7 @@
         return w.at[:, rows(side, height, h), :]
 
     def send_weights(height, send, recv, device):
-        remote(wt.at[:, span(r * hr, hr, hr), units(height)], piece(y, z, r), send, recv, device).start()
+        remote(wt.at[:, :, units(height)], piece(y, z, r), send, recv, device).start()
 
     def wx(k, a, block):
         return remote(block, block, wxs.at[0], wxr.at[k, a], to_x)
@@ -160,7 +163,7 @@
         for d in range(2):
             origin, target = z - step_of(d) * k, z + step_of(d)
             block = block_of(g, origin, t)
-            ahead = remote(block, block, ags.at[g, min(k, last - 1), d], agr.at[g, origin], layer(target))
+            ahead = remote(block, block, ags.at[g, max(min(k, last - 1) - 1, 0), d], agr.at[g, origin], layer(target))
             chosen = exists(origin)
             if ends is not None:
                 at_end = origin == (last if d else 0)
@@ -391,6 +394,8 @@
     def send_first():
         for copy in local_weights:
             copy.wait()
+        for copy in local_tokens:
+            copy.start()
         for k in range(1, nz):
             send_weights(flip(z, k, nz), wzs.at[0], wzr.at[k], layer(flip(z, k, nz)))
         send_weights(z, wys.at[0], wyr.at[0, 0], to_y)
@@ -399,6 +404,8 @@
         send_own(EARLY)
         send_own(COT)
         send_own(LATE, True)
+        for copy in local_own + local_sums:
+            copy.start()
         for copy in local_own:
             copy.wait()
 
@@ -602,7 +609,7 @@
         out_specs=(VMEM,) * 5,
         scratch_shapes=[
             pltpu.VMEM((3, nz, m, width), bf16),
-            pltpu.VMEM((3, dl, ff), bf16),
+            pltpu.VMEM((3, hr, ff), bf16),
             pltpu.VMEM((3, width, u), bf16),
             pltpu.VMEM((3, dl, ff), bf16),
             pltpu.VMEM((3, nz, m, u), bf16),
@@ -621,7 +628,7 @@
         ]
         + [dma(3)] * 4
         + [dma(1), dma(nz), dma(1), dma(nz, 2), dma(1), dma(nz, 2)]
-        + [dma(3, 2), dma(3, max(nz - 1, 1), 2), dma(3, nz), dma(1), dma(3, nz)]
+        + [dma(3, 2), dma(3, max(nz - 2, 1), 2), dma(3, nz), dma(1), dma(3, nz)]
         + [dma(1), dma(2, nz), dma(1), dma(2, 2, nz), dma(2), dma(2)]
         + [dma(1), dma(nz, 3)] * 4,
         compiler_params=pltpu.CompilerParams(

time: 136 us -> 134 us (0.985)
  Pallas kernels: 135 us -> 133 us
    pallas_call x1, Pallas kernels: 132 us -> 130 us  [split_hidden(): pl.pallas_call(functools.partial(fused_kernel, nz), out_shape=(jax.ShapeD...]
where the time goes in v5:
time: 134 us
  Pallas kernels  133 us (99%)
    pallas_call x1, Pallas kernels, split_hidden(): pl.pallas_call(functools.partial(fused_kernel, nz), out_shape=(jax.ShapeD...  130 us

profile of v5, /device:TPU:0, one launch (start us, length us, event | category | flops | bytes accessed | tf_op | source)
XLA Modules:
  0.0 133.6 jit_solution(8563465611398479583)
XLA Ops:
  0.6 130.2 %fused.1 = (bf16[128,2048]{1,0:T(8,128)(2,1)S(1)}, bf16[128,2048]{1,0:T(8,128)(2,1)S(1)}, f32[256,1536]{1,0:T(8,128)S(1)}, f32[256,1536]{1,0:T(8,128)S(1)}, f32[256,1536]{1,0:T(8,128)S(1)}) custom-call(bf16[128,2048]{1,0:T(8,128)(2,1)} %later.1, bf16[128,2048]{1,0:T(8,128)(2,1)} %earlier.1, bf16[128,2048]{1,0:T(8,128)(2,1)} %cot.1, bf16[256,1536]{1,0:T(8,128)(2,1)} %gw.1, ...), custom_call_target="tpu_custom_call" | custom-call | tf_op jit(solution)/shard_map/fused/pallas_call | solution.py:599
  130.9 2.6 %close.1 = (bf16[128,2048]{1,0:T(8,128)(2,1)}, bf16[128,2048]{1,0:T(8,128)(2,1)}, f32[256,1536]{1,0:T(8,128)}, f32[256,1536]{1,0:T(8,128)}, f32[256,1536]{1,0:T(8,128)}) custom-call(bf16[128,2048]{1,0:T(8,128)(2,1)S(1)} %get-tuple-element.10.refs_0_, bf16[128,2048]{1,0:T(8,128)(2,1)S(1)} %get-tuple-element.11.refs_1_, ...), custom_call_target="tpu_custom_call" | custom-call | tf_op jit(solution)/shard_map/close/pallas_call | solution.py:563

commit v6 on v5

--- a/solution.py
+++ b/solution.py
@@ -497,8 +497,8 @@
             place(5 + 2 * (last - far) + 5 * (h - 1), "sum_l", sum_step, 0, far, h)
     for c, (k, i) in enumerate(crossing):
         if c > 1:
-            place(c, "cross_send", cross_send, k, i, c)
-        place((0, 2, 5, 6, 7, 8)[c], "cross_turn", cross_turn, k, i, c)
+            place(c - 2, "cross_send", cross_send, k, i, c)
+        place((0, 2, 4, 5, 7, 8)[c], "cross_turn", cross_turn, k, i, c)
         place((6, 7, 8, 8, 9, 9)[c], "cross_end", cross_end, k, i, c)
         if k:
             place((6, 7, 8, 8, 9, 9)[c] + 3, "grad_back", grad_back, k, i)

time: 134 us -> 133 us (level)
  no operation moved by 1% of the time
where the time goes in v6:
time: 133 us
  Pallas kernels  132 us (99%)
    pallas_call x1, Pallas kernels, split_hidden(): pl.pallas_call(functools.partial(fused_kernel, nz), out_shape=(jax.ShapeD...  129 us

profile of v6, /device:TPU:0, one launch (start us, length us, event | category | flops | bytes accessed | tf_op | source)
XLA Modules:
  0.0 132.9 jit_solution(4851888724267488001)
XLA Ops:
  0.6 129.5 %fused.1 = (bf16[128,2048]{1,0:T(8,128)(2,1)S(1)}, bf16[128,2048]{1,0:T(8,128)(2,1)S(1)}, f32[256,1536]{1,0:T(8,128)S(1)}, f32[256,1536]{1,0:T(8,128)S(1)}, f32[256,1536]{1,0:T(8,128)S(1)}) custom-call(bf16[128,2048]{1,0:T(8,128)(2,1)} %later.1, bf16[128,2048]{1,0:T(8,128)(2,1)} %earlier.1, bf16[128,2048]{1,0:T(8,128)(2,1)} %cot.1, bf16[256,1536]{1,0:T(8,128)(2,1)} %gw.1, ...), custom_call_target="tpu_custom_call" | custom-call | tf_op jit(solution)/shard_map/fused/pallas_call | solution.py:599
  130.1 2.6 %close.1 = (bf16[128,2048]{1,0:T(8,128)(2,1)}, bf16[128,2048]{1,0:T(8,128)(2,1)}, f32[256,1536]{1,0:T(8,128)}, f32[256,1536]{1,0:T(8,128)}, f32[256,1536]{1,0:T(8,128)}) custom-call(bf16[128,2048]{1,0:T(8,128)(2,1)S(1)} %get-tuple-element.10.refs_0_, bf16[128,2048]{1,0:T(8,128)(2,1)S(1)} %get-tuple-element.11.refs_1_, ...), custom_call_target="tpu_custom_call" | custom-call | tf_op jit(solution)/shard_map/close/pallas_call | solution.py:563
